TPU v7x, 128 devices: a whole 4x4x4 slice. The times are simulated.
128 devices in a mesh: ep: 64 (over z, y, x), tp: 2 (over core).
Axes of the slice: x: 4, y: 4, z: 4, core: 2. Of those that a mesh axis runs over, the one named last changes fastest.
Arguments:
- residual: bfloat16 [4096, 2048], P('ep', 'tp'), may hold values from -100 to 100
- route_ids: int32 [4096, 4], P('ep'), may hold values from 0 to 63, all different within a row; in each aligned block of 64 rows (0 to 63, 64 to 127, ...) at most 6 rows name the same one
- route_weights: float32 [4096, 4], P('ep'), may hold values from 0.1 to 1
- carried_state: float32 [2, 4096, 4096], P(None, 'ep', 'tp'), may hold values from -6 to 6
- mix_gain: float32 [2048], replicated, may hold values from 0.1 to 1.9
- in_proj: bfloat16 [2048, 1024], P(None, 'tp'), may hold values from -0.125 to 0.125
- decay_rate: float32 [64, 64], P('tp'), may hold values from 0.1 to 2
- frequency: float32 [64, 64], P('tp'), may hold values from -3 to 3
- step_size: float32 [64], P('tp'), may hold values from 0.05 to 1
- input_map: float32 [2, 64, 64, 16], P(None, 'tp'), may hold values from -1.5 to 1.5
- output_matrix: float32 [2, 64, 16, 64], P(None, 'tp'), may hold values from -0.5 to 0.5
- passthrough_scale: float32 [1024], P('tp'), may hold values from -4 to 4
- out_gain: float32 [1024], replicated, may hold values from 0.1 to 1.9
- out_proj: bfloat16 [1024, 2048], P(None, 'tp'), may hold values from -0.1875 to 0.1875
- ffn_gain: float32 [2048], replicated, may hold values from 0.1 to 1.9
- w_gate: bfloat16 [64, 2048, 2048], P('ep', None, 'tp'), may hold values from -5 to 5
- w_up: bfloat16 [64, 2048, 2048], P('ep', None, 'tp'), may hold values from -5 to 5
- w_down: bfloat16 [64, 2048, 2048], P('ep', 'tp'), may hold values from -0.125 to 0.125
Outputs:
- updated: bfloat16 [4096, 2048], P('ep', 'tp')
- new_state: float32 [2, 4096, 4096], P(None, 'ep', 'tp')
Inputs may be any that keep to these rules, and one draw needn't show every extreme that they name: `route_ids`: each row names 4 different experts. Among the 64 rows of one device (aligned blocks) no expert is named more than 6 times, and in every draw some block names some expert exactly 6 times.
All inputs are finite; a program needn't handle non-finite values.
Results may differ from a plain program's by a relative error of at most 0.018.
Values may be sent and summed in bfloat16 or wider, within the bound.
A program may use at most 128 MiB of HBM per device.

v0:
```python
import jax
import jax.numpy as jnp
from jax import lax
from jax.sharding import PartitionSpec as P

epsilon = 1e-06
clamp_limit = 7.0
swish_alpha = 1.702


def from_everyone(array, axis):
    peers = lax.axis_size(axis)
    return lax.all_to_all(
        jnp.broadcast_to(array[None], (peers, *array.shape)), axis, 0, 0, tiled=True
    )


def joined_along(tiles, dim):
    tiles = jnp.moveaxis(tiles, 0, dim)
    dims = tiles.shape
    return tiles.reshape(*dims[:dim], dims[dim] * dims[dim + 1], *dims[dim + 2 :])


def gather_directly(array, axis, dim):
    tiles = from_everyone(array, axis)
    return joined_along(tiles, dim)


def in_blocks(array, dim, peers):
    dims = array.shape
    tiles = array.reshape(*dims[:dim], peers, dims[dim] // peers, *dims[dim + 1 :])
    return jnp.moveaxis(tiles, dim, 0)


def sum_at_owner(array, axis, dim):
    peers = lax.axis_size(axis)
    tiles = lax.all_to_all(in_blocks(array, dim, peers), axis, 0, 0, tiled=True)
    return jnp.sum(tiles.astype(jnp.float32), axis=0)


def rms_rows(values, gain_vec):
    return values * lax.rsqrt(jnp.mean(values * values, axis=1, keepdims=True) + epsilon) * gain_vec


def discretize(decay_rate, frequency, step_size):
    rate_real = -decay_rate
    time_step = step_size[:, None]
    magnitude = jnp.exp(rate_real * time_step)
    phase_angle = frequency * time_step
    bar_real = magnitude * jnp.cos(phase_angle)
    bar_imag = magnitude * jnp.sin(phase_angle)
    denominator = rate_real * rate_real + frequency * frequency
    shifted = bar_real - 1.0
    coef_real = (shifted * rate_real + bar_imag * frequency) / denominator
    coef_imag = (bar_imag * rate_real - shifted * frequency) / denominator
    return (bar_real, bar_imag, coef_real, coef_imag)


def state_step(
    channels,
    carried_state,
    decay_rate,
    frequency,
    step_size,
    input_map,
    output_matrix,
    passthrough_scale,
):
    row_count = channels.shape[0]
    number_of_groups, state_width = decay_rate.shape
    channels_per_group = input_map.shape[3]
    bar_real, bar_imag, coef_real, coef_imag = discretize(decay_rate, frequency, step_size)
    map_real = coef_real[..., None] * input_map[0] - coef_imag[..., None] * input_map[1]
    map_imag = coef_real[..., None] * input_map[1] + coef_imag[..., None] * input_map[0]
    input_rows = channels.astype(jnp.float32).reshape(
        row_count, number_of_groups, channels_per_group
    )
    push_real = jnp.einsum("sgc,gpc->sgp", input_rows, map_real)
    push_imag = jnp.einsum("sgc,gpc->sgp", input_rows, map_imag)
    old_real = carried_state[0].reshape(row_count, number_of_groups, state_width)
    old_imag = carried_state[1].reshape(row_count, number_of_groups, state_width)
    updated_real = bar_real * old_real - bar_imag * old_imag + push_real
    updated_imaginary = bar_real * old_imag + bar_imag * old_real + push_imag
    mixer_output = (
        jnp.einsum("dfk,idk->idf", output_matrix[0], updated_real)
        - jnp.einsum("dfk,idk->idf", output_matrix[1], updated_imaginary)
        + passthrough_scale.reshape(number_of_groups, channels_per_group) * input_rows
    )
    activated = jax.nn.gelu(
        mixer_output.reshape(row_count, number_of_groups * channels_per_group)
    ).astype(jnp.bfloat16)
    new_state = jnp.stack(
        [updated_real.reshape(row_count, -1), updated_imaginary.reshape(row_count, -1)]
    )
    return (activated, new_state)


def own_slice(vector, width):
    return lax.dynamic_slice_in_dim(vector, lax.axis_index("tp") * width, width)


def local(
    residual,
    route_ids,
    route_weights,
    carried_state,
    mix_gain,
    in_proj,
    decay_rate,
    frequency,
    step_size,
    input_map,
    output_matrix,
    passthrough_scale,
    out_gain,
    out_proj,
    ffn_gain,
    w_gate,
    w_up,
    w_down,
):
    row_count, half_width = residual.shape
    top_count = route_ids.shape[1]
    local_experts = w_gate.shape[0]
    peer_count = lax.axis_size("ep")
    expert_count = local_experts * peer_count
    capacity = max(2, 3 * row_count * top_count // (2 * expert_count))
    whole_rows = lax.all_gather(residual, "tp", axis=1, tiled=True)
    normed_rows = rms_rows(whole_rows.astype(jnp.float32), mix_gain).astype(jnp.bfloat16)
    channels = jnp.dot(normed_rows, in_proj, preferred_element_type=jnp.float32).astype(
        jnp.bfloat16
    )
    activated, new_state = state_step(
        channels,
        carried_state,
        decay_rate,
        frequency,
        step_size,
        input_map,
        output_matrix,
        passthrough_scale,
    )
    channel_width = activated.shape[1]
    own_half = activated.astype(jnp.float32)
    total_sq = lax.psum(jnp.sum(own_half * own_half, axis=1), "tp")
    full_width = channel_width * lax.axis_size("tp")
    row_scale = lax.rsqrt(total_sq / full_width + epsilon)[:, None]
    local_scaled = (own_half * row_scale * own_slice(out_gain, channel_width)).astype(jnp.bfloat16)
    scaled = gather_directly(local_scaled, "tp", 1)
    after_mixer = (
        residual.astype(jnp.float32) + jnp.dot(scaled, out_proj, preferred_element_type=jnp.float32)
    ).astype(jnp.bfloat16)
    flat_ids = route_ids.reshape(row_count * top_count)
    onehot = (flat_ids[:, None] == jnp.arange(expert_count, dtype=jnp.int32)[None, :]).astype(
        jnp.int32
    )
    before = jnp.cumsum(onehot, axis=0) - onehot
    slot_index = jnp.sum(before * onehot, axis=1)
    position = flat_ids * capacity + slot_index
    slot_table = jnp.any(
        jnp.arange(expert_count * capacity, dtype=jnp.int32)[:, None, None]
        == position.reshape(row_count, top_count)[None, :, :],
        axis=2,
    ).astype(jnp.bfloat16)
    own_half = after_mixer.astype(jnp.float32)
    total_sq = lax.psum(jnp.sum(own_half * own_half, axis=1), "tp")
    full_width = half_width * lax.axis_size("tp")
    row_scale = lax.rsqrt(total_sq / full_width + epsilon)[:, None]
    expert_in = (own_half * row_scale * own_slice(ffn_gain, half_width)).astype(jnp.bfloat16)
    buffer = jnp.dot(slot_table, expert_in, preferred_element_type=jnp.float32).astype(jnp.bfloat16)
    buffer = buffer.reshape(peer_count, local_experts, capacity, half_width)
    arrived = gather_directly(
        lax.all_to_all(buffer, "ep", split_axis=0, concat_axis=0, tiled=True), "tp", 3
    )
    gate_pre = jnp.einsum("necd,edf->necf", arrived, w_gate, preferred_element_type=jnp.float32)
    up_pre = jnp.einsum("necd,edf->necf", arrived, w_up, preferred_element_type=jnp.float32)
    gated = jnp.minimum(gate_pre, clamp_limit)
    activation = (
        (jnp.clip(up_pre, -clamp_limit, clamp_limit) + 1.0)
        * gated
        * jax.nn.sigmoid(swish_alpha * gated)
    ).astype(jnp.bfloat16)
    partial_value = jnp.einsum(
        "necf,efd->necd", activation, w_down, preferred_element_type=jnp.float32
    )
    partial_value = lax.optimization_barrier(partial_value.astype(jnp.bfloat16)).astype(jnp.float32)
    summed = sum_at_owner(partial_value.astype(jnp.bfloat16), "tp", 3).astype(jnp.bfloat16)
    result = lax.all_to_all(summed, "ep", split_axis=0, concat_axis=0, tiled=True)
    returned = result.reshape(expert_count * capacity, half_width)
    picked = returned[position].reshape(row_count, top_count, half_width)
    expert_sum = jnp.sum(route_weights[:, :, None] * picked.astype(jnp.float32), axis=1)
    updated = (after_mixer.astype(jnp.float32) + expert_sum).astype(jnp.bfloat16)
    return (updated, new_state)


def solution(mesh):
    placed = (
        P("ep", "tp"),
        P("ep", None),
        P("ep", None),
        P(None, "ep", "tp"),
        P(),
        P(None, "tp"),
        P("tp", None),
        P("tp", None),
        P("tp"),
        P(None, "tp", None, None),
        P(None, "tp", None, None),
        P("tp"),
        P(),
        P(None, "tp"),
        P(),
        P("ep", None, "tp"),
        P("ep", None, "tp"),
        P("ep", "tp", None),
    )
    return jax.shard_map(
        local,
        mesh=mesh,
        in_specs=placed,
        out_specs=(P("ep", "tp"), P(None, "ep", "tp")),
        check_vma=False,
    )
```

profile of v0, /device:TPU:1, one launch (start us, length us, event | category | flops | bytes accessed | tf_op | source)
XLA Modules:
  0.0 133.3 jit_solution(11840275723541302915)
XLA Ops:
  0.7 3.4 %all_gather.3 = bf16[64,2048]{1,0:T(8,128)(2,1)S(1)} all-gather(bf16[64,1024]{1,0:T(8,128)(2,1)} %param.18), channel_id=1, replica_groups=mesh['ep'=64,'tp'=2] {'tp'}, dimensions={1}, use_global_device_ids=true | all-gather | bytes 393216 | tf_op jit(solution)/shard_map/all_gather | solution.py:128
  4.2 2.1 %convolution_convert_fusion.1 = bf16[64,512]{1,0:T(8,128)(2,1)S(1)} fusion(bf16[2048,512]{1,0:T(8,128)(2,1)} %param.23, bf16[64,2048]{1,0:T(8,128)(2,1)S(1)} %all_gather.3, f32[2048]{0:T(1024)} %param.22, f32[64]{0:T(128)S(1)} %add_rsqrt_fusion.2), kind=kOutput, calls=%fused_computation.22 | convolution fusion | flops 134774784 | bytes 2433280 | tf_op jit(solution)/shard_map/dot_general | solution.py:130
  6.5 1.0 fusion.77
  7.5 1.4 %copy.109 = f32[1,64,2048]{1,2,0:T(8,128)S(1)} copy(f32[1,64,2048]{2,1,0:T(8,128)} %get-tuple-element.2) | data formatting | bytes 1048576 | tf_op jit(solution)/shard_map/slice | solution.py:80
  8.9 2.4 %copy.110 = f32[1,64,2048]{1,2,0:T(8,128)} copy(f32[1,64,2048]{2,1,0:T(8,128)} %get-tuple-element.3) | data formatting | bytes 1048576 | tf_op jit(solution)/shard_map/slice | solution.py:81
  11.4 3.3 %fusion.15 = f32[64,32,64]{0,2,1:T(8,128)} fusion(bf16[64,32,16]{0,2,1:T(8,128)(2,1)S(1)} %bitcast.128, f32[64,32,64]{0,2,1:T(8,128)S(1)} %bitcast.117, f32[64,32,64]{0,2,1:T(8,128)} %bitcast.119, f32[32,64]{1,0:T(8,128)S(1)} %get-tuple-element.7, f32[32,64]{1,0:T(8,128)S(1)} %get-tuple-element.5, f32[2,32,64,16]{2,3,1,0:T(8,128)} %param.27, ...), kind=kOutput, calls=%fused_computation.15 | convolution fusion | flops 4816896 | bytes 1933312 | tf_op jit(solution)/shard_map/sgc,gpc->sgp/dot_general | solution.py:79
  14.8 1.8 %fusion.14 = f32[64,32,64]{0,2,1:T(8,128)} fusion(bf16[64,32,16]{0,2,1:T(8,128)(2,1)S(1)} %bitcast.129, f32[64,32,64]{0,2,1:T(8,128)S(1)} %bitcast.120, f32[64,32,64]{0,2,1:T(8,128)S(1)} %bitcast.118, f32[32,64]{1,0:T(8,128)S(1)} %get-tuple-element.7, f32[32,64]{1,0:T(8,128)S(1)} %get-tuple-element.5, f32[2,32,64,16]{2,3,1,0:T(8,128)S(1)} %copy-done.5, ...), kind=kOutput, calls=%fused_computation.14 | convolution fusion | flops 4816896 | bytes 1933312 | tf_op jit(solution)/shard_map/sgc,gpc->sgp/dot_general | solution.py:78
  16.6 1.6 %fusion.40 = f32[32,64,16]{1,2,0:T(8,128)S(1)} fusion(f32[64,32,64]{0,2,1:T(8,128)} %fusion.14, f32[2,32,16,64]{3,2,1,0:T(8,128)} %param.28), kind=kOutput, calls=%fused_computation.46 | convolution fusion | flops 4194304 | bytes 1310720 | tf_op jit(solution)/shard_map/dfk,idk->idf/dot_general | solution.py:85
  18.3 0.8 multiply_reduce_fusion.2
  19.1 2.6 %psum.14 = f32[64]{0:T(128)S(1)} all-reduce(f32[64]{0:T(128)} %get-tuple-element.10), channel_id=1, replica_groups=mesh['ep'=64,'tp'=2] {'tp'}, use_global_device_ids=true, to_apply=%region_2.0 | all-reduce | flops 64 | bytes 512 | tf_op jit(solution)/shard_map/psum | solution.py:145
  23.4 3.7 %all-to-all-start = ((bf16[2,64,512]{2,1,0:T(8,128)(2,1)}), bf16[2,64,512]{2,1,0:T(8,128)(2,1)S(1)}, u32[]{:S(2)}, u32[]{:S(2)}) async-start(bf16[2,64,512]{2,1,0:T(8,128)(2,1)} %broadcast_in_dim.6), calls=%async_computation | async-start | bytes 262144 | tf_op jit(solution)/shard_map/all_to_all | solution.py:13
  30.0 2.5 %psum.15 = f32[64]{0:T(128)S(1)} all-reduce(f32[64]{0:T(128)S(1)} %get-tuple-element.12), channel_id=1, replica_groups=mesh['ep'=64,'tp'=2] {'tp'}, use_global_device_ids=true, to_apply=%region_8.9 | all-reduce | flops 64 | bytes 512 | tf_op jit(solution)/shard_map/psum | solution.py:166
  32.5 1.3 convolution_convert_fusion
  33.8 1.3 %reshape.193 = bf16[64,1,6,1024]{3,2,0,1:T(8,128)(2,1)S(1)} reshape(bf16[384,1024]{1,0:T(8,128)(2,1)} %convolution_convert_fusion) | data formatting | bytes 1572864 | tf_op jit(solution)/shard_map/reshape | solution.py:171
  35.2 29.2 %all_to_all.25 = bf16[64,1,6,1024]{3,2,1,0:T(8,128)(2,1)S(1)} all-to-all(bf16[64,1,6,1024]{3,2,1,0:T(8,128)(2,1)S(1)} %bitcast.125), channel_id=1, replica_groups=mesh['ep'=64,'tp'=2] {'ep'}, dimensions={0} | all-to-all | bytes 1572864 | tf_op jit(solution)/shard_map/all_to_all | solution.py:173
  65.0 6.4 %all_to_all.26 = bf16[2,64,1,6,1024]{4,1,3,2,0:T(8,128)(2,1)S(1)} all-to-all(bf16[2,64,1,6,1024]{4,1,3,2,0:T(8,128)(2,1)S(1)} %broadcast_in_dim.8), channel_id=1, replica_groups=mesh['ep'=64,'tp'=2] {'tp'}, dimensions={0} | all-to-all | bytes 3145728 | tf_op jit(solution)/shard_map/all_to_all | solution.py:13
  71.4 2.8 %copy.128 = bf16[64,1,6,2,1024]{4,3,0,2,1:T(2,128)(2,1)} copy(bf16[64,1,6,2,1024]{4,0,2,1,3:T(8,128)(2,1)S(1)} %bitcast.123) | data formatting | bytes 3145728 | tf_op jit(solution)/shard_map/transpose | solution.py:19
  74.1 3.9 %reshape.194 = bf16[64,6,2048]{2,0,1:T(8,128)(2,1)} reshape(bf16[64,1,6,2,1024]{4,3,0,2,1:T(2,128)(2,1)} %copy.128) | data formatting | bytes 3145728 | tf_op jit(solution)/shard_map/reshape.5
  78.0 5.6 %fusion.2 = f32[64,6,1024]{2,0,1:T(8,128)} fusion(bf16[64,6,2048]{2,0,1:T(8,128)(2,1)} %reshape.194, bf16[1,2048,1024]{2,1,0:T(8,128)(2,1)} %param.33), kind=kOutput, calls=%fused_computation.3 | convolution fusion | flops 1610612736 | bytes 7340032 | tf_op jit(solution)/shard_map/necd,edf->necf/dot_general | solution.py:175
  83.6 9.2 %fusion.9 = bf16[64,1,6,2048]{3,0,2,1:T(8,128)(2,1)} fusion(bf16[1,1024,2048]{2,1,0:T(8,128)(2,1)} %param.35, f32[64,6,1024]{2,0,1:T(8,128)} %fusion.2, bf16[64,6,2048]{2,0,1:T(8,128)(2,1)} %reshape.194, bf16[1,2048,1024]{2,1,0:T(8,128)(2,1)} %param.34), kind=kOutput, calls=%fused_computation.8 | convolution fusion | flops 3225944064 | bytes 13107200 | tf_op jit(solution)/shard_map/necf,efd->necd/dot_general | solution.py:183
  92.8 1.5 %copy.142 = bf16[1,6,8,2,8,1024]{5,4,2,1,0,3:T(8,128)(2,1)S(1)} copy(bf16[1,6,8,2,8,1024]{5,4,3,2,1,0:T(8,128)(2,1)} %bitcast.131) | data formatting | bytes 3145728 | tf_op jit(solution)/shard_map/reshape | solution.py:31
  94.4 5.8 %all_to_all.27 = bf16[2,64,1,6,1024]{4,1,3,2,0:T(8,128)(2,1)} all-to-all(bf16[2,64,1,6,1024]{4,1,3,2,0:T(8,128)(2,1)S(1)} %bitcast.124), channel_id=1, replica_groups=mesh['ep'=64,'tp'=2] {'tp'}, dimensions={0} | all-to-all | bytes 3145728 | tf_op jit(solution)/shard_map/all_to_all | solution.py:37
  100.2 1.8 %reduce_sum.68 = bf16[64,6,1024]{2,0,1:T(8,128)(2,1)S(1)} reduce(bf16[2,64,1,6,1024]{4,1,3,2,0:T(8,128)(2,1)} %all_to_all.27, bf16[]{:T(256)} %constant.55.clone.1), dimensions={0,2}, to_apply=%region_9.10 | reduce | flops 393216 | bytes 2359298 | tf_op jit(solution)/shard_map/reduce_sum | solution.py:38
  102.0 1.5 %copy.131 = bf16[64,1,6,1024]{3,2,1,0:T(8,128)(2,1)} copy(bf16[64,1,6,1024]{3,0,2,1:T(8,128)(2,1)S(1)} %bitcast.127) | data formatting | bytes 1572864 | tf_op jit(solution)/shard_map/reduce_sum | solution.py:38
  103.5 5.6 %all-to-all-start.4 = ((bf16[64,1,6,1024]{3,2,1,0:T(8,128)(2,1)}), bf16[64,1,6,1024]{3,2,1,0:T(8,128)(2,1)}, u32[]{:S(2)}, u32[]{:S(2)}) async-start(bf16[64,1,6,1024]{3,2,1,0:T(8,128)(2,1)} %copy.131), calls=%async_computation.4 | async-start | bytes 2097152 | tf_op jit(solution)/shard_map/all_to_all | solution.py:188
  109.3 2.3 %copy.133 = f32[1,64,2048]{2,1,0:T(8,128)} copy(f32[1,64,2048]{1,2,0:T(8,128)} %bitcast.122) | data formatting | bytes 1048576 | tf_op jit(solution)/shard_map/stack;reshape | solution.py:92
  111.7 1.1 copy.132
  112.8 2.3 %pad_maximum_fusion = f32[2,64,2048]{2,1,0:T(8,128)} fusion(f32[1,64,2048]{2,1,0:T(8,128)} %copy.133, f32[1,64,2048]{2,1,0:T(8,128)} %copy.132), kind=kLoop, calls=%fused_computation.23 | loop fusion | flops 262144 | bytes 2097152 | tf_op jit(solution)/shard_map/stack | solution.py:92
  115.1 12.0 %all-to-all-done.4 = bf16[64,1,6,1024]{3,2,1,0:T(8,128)(2,1)} async-done(((bf16[64,1,6,1024]{3,2,1,0:T(8,128)(2,1)}), bf16[64,1,6,1024]{3,2,1,0:T(8,128)(2,1)}, u32[]{:S(2)}, u32[]{:S(2)}) %all-to-all-start.4) | async-done | bytes 786464 | tf_op jit(solution)/shard_map/all_to_all | solution.py:188
  127.1 1.4 %reshape.200 = bf16[384,1024]{1,0:T(8,128)(2,1)S(1)} reshape(bf16[64,1,6,1024]{3,2,1,0:T(8,128)(2,1)} %all-to-all-done.4) | data formatting | bytes 1572864 | tf_op jit(solution)/shard_map/reshape | solution.py:189
  128.5 2.0 %gather_fusion = bf16[256,1024]{1,0:T(8,128)(2,1)} fusion(bf16[384,1024]{1,0:T(8,128)(2,1)S(1)} %reshape.200, s32[1024]{0:T(1024)S(1)} %pad_clamp_fusion), kind=kCustom, calls=%fused_computation | custom fusion | bytes 1049600 | tf_op jit(solution)/shard_map/gather | solution.py:190
  130.5 1.4 %reshape.202 = f32[64,4,1024]{2,1,0:T(4,128)S(1)} reshape(bf16[256,1024]{1,0:T(8,128)(2,1)} %gather_fusion) | data formatting | bytes 1572864 | tf_op jit(solution)/shard_map/convert_element_type | solution.py:191
  (64 shorter events, 7.4 us)
Async XLA Ops:
  0.6 28.8 %copy-start = (bf16[1024,1024]{1,0:T(8,128)(2,1)S(1)}, bf16[1024,1024]{1,0:T(8,128)(2,1)}, u32[]{:S(2)}) copy-start(bf16[1024,1024]{1,0:T(8,128)(2,1)} %param.31) | copy-start | bytes 6291460
  0.6 5.8 %copy-start.4 = (f32[2,64,2048]{2,1,0:T(8,128)S(1)}, f32[2,64,2048]{2,1,0:T(8,128)}, u32[]{:S(2)}) copy-start(f32[2,64,2048]{2,1,0:T(8,128)} %param.21) | copy-start | bytes 3145732
  7.5 3.8 %copy-start.8 = (f32[32,64]{1,0:T(8,128)S(1)}, f32[32,64]{1,0:T(8,128)}, u32[]{:S(2)}) copy-start(f32[32,64]{1,0:T(8,128)} %param.25) | copy-start | bytes 24580
  7.5 3.8 %copy-start.9 = (f32[32,64]{1,0:T(8,128)S(1)}, f32[32,64]{1,0:T(8,128)}, u32[]{:S(2)}) copy-start(f32[32,64]{1,0:T(8,128)} %param.24) | copy-start | bytes 24580
  7.5 3.8 %copy-start.13 = (f32[32]{0:T(128)S(1)}, f32[32]{0:T(128)}, u32[]{:S(2)}) copy-start(f32[32]{0:T(128)} %param.26) | copy-start | bytes 388
  11.4 3.3 %copy-start.1 = (f32[1,64,2048]{1,2,0:T(8,128)S(1)}, f32[1,64,2048]{1,2,0:T(8,128)}, u32[]{:S(2)}) copy-start(f32[1,64,2048]{1,2,0:T(8,128)} %copy.110) | copy-start | bytes 1572868
  11.4 3.3 %copy-start.5 = (f32[2,32,64,16]{2,3,1,0:T(8,128)S(1)}, f32[2,32,64,16]{2,3,1,0:T(8,128)}, u32[]{:S(2)}) copy-start(f32[2,32,64,16]{2,3,1,0:T(8,128)} %param.27) | copy-start | bytes 786436
  14.8 1.8 %copy-start.10 = (f32[512]{0:T(512)S(1)}, f32[512]{0:T(512)}, u32[]{:S(2)}) copy-start(f32[512]{0:T(512)} %param.29) | copy-start | bytes 6148
  16.6 1.7 %copy-start.3 = (f32[64,32,64]{0,2,1:T(8,128)S(1)}, f32[64,32,64]{0,2,1:T(8,128)}, u32[]{:S(2)}) copy-start(f32[64,32,64]{0,2,1:T(8,128)} %fusion.15) | copy-start | bytes 1572868
  16.6 1.7 %copy-start.7 = (f32[2,32,16,64]{3,2,1,0:T(8,128)S(1)}, f32[2,32,16,64]{3,2,1,0:T(8,128)}, u32[]{:S(2)}) copy-start(f32[2,32,16,64]{3,2,1,0:T(8,128)} %param.28) | copy-start | bytes 786436
  19.1 10.3 %copy-start.6 = (bf16[64,1024]{1,0:T(8,128)(2,1)S(1)}, bf16[64,1024]{1,0:T(8,128)(2,1)}, u32[]{:S(2)}) copy-start(bf16[64,1024]{1,0:T(8,128)(2,1)} %param.18) | copy-start | bytes 393220
  23.4 6.0 %all-to-all-start = ((bf16[2,64,512]{2,1,0:T(8,128)(2,1)}), bf16[2,64,512]{2,1,0:T(8,128)(2,1)S(1)}, u32[]{:S(2)}, u32[]{:S(2)}) async-start(bf16[2,64,512]{2,1,0:T(8,128)(2,1)} %broadcast_in_dim.6), calls=%async_computation | async-start | bytes 262144 | tf_op jit(solution)/shard_map/all_to_all | solution.py:13
  29.0 3.5 %copy-start.12 = (f32[2048]{0:T(1024)S(1)}, f32[2048]{0:T(1024)}, u32[]{:S(2)}) copy-start(f32[2048]{0:T(1024)} %param.32) | copy-start | bytes 24580
  102.0 7.1 %copy-start.11 = (f32[64,4]{0,1:T(4,128)S(1)}, f32[64,4]{0,1:T(4,128)}, u32[]{:S(2)}) copy-start(f32[64,4]{0,1:T(4,128)} %param.20) | copy-start | bytes 3076
  103.5 8.2 %copy-start.2 = (f32[64,32,64]{0,2,1:T(8,128)S(1)}, f32[64,32,64]{0,2,1:T(8,128)}, u32[]{:S(2)}) copy-start(f32[64,32,64]{0,2,1:T(8,128)} %fusion.14) | copy-start | bytes 1572868
  103.5 23.7 %all-to-all-start.4 = ((bf16[64,1,6,1024]{3,2,1,0:T(8,128)(2,1)}), bf16[64,1,6,1024]{3,2,1,0:T(8,128)(2,1)}, u32[]{:S(2)}, u32[]{:S(2)}) async-start(bf16[64,1,6,1024]{3,2,1,0:T(8,128)(2,1)} %copy.131), calls=%async_computation.4 | async-start | bytes 2097152 | tf_op jit(solution)/shard_map/all_to_all | solution.py:188
where the time goes:
time: 134 us; the launch traced here: 133 us
  blocking collectives  49.8 us (37%)
  local copies, waits for them, and re-layouts  28 us (21%)
  matrix products  26.4 us (20%)
  waiting for transfers between devices  12 us (9%)
  starting transfers between devices  9.35 us (7%)
  other arithmetic  6.82 us (5%)
    all_to_all x1, blocking collectives, local(): lax.all_to_all(buffer, 'ep', split_axis=0, concat_axis=0, tiled=True)  29.2 us
    all_to_all x1, waiting for transfers between devices, local(): lax.all_to_all(summed, 'ep', split_axis=0, concat_axis=0, tiled=True)  12 us
    dot_general x1, matrix products, local(): jnp.einsum('necf,efd->necd', activation, w_down, preferred_element_type=j...  9.23 us
    all_to_all x1, blocking collectives, from_everyone(): lax.all_to_all(jnp.broadcast_to(array[None], (peers, *array.shape)), axis...  6.37 us
    all_to_all x1, blocking collectives, sum_at_owner(): tiles = lax.all_to_all(in_blocks(array, dim, peers), axis, 0, 0, tiled=True)  5.77 us
    all_to_all x1, starting transfers between devices, local(): lax.all_to_all(summed, 'ep', split_axis=0, concat_axis=0, tiled=True)  5.64 us
    dot_general x1, matrix products, local(): jnp.einsum('necd,edf->necf', arrived, w_gate, preferred_element_type=jnp....  5.6 us
    psum x2, blocking collectives, local(): total_sq = lax.psum(jnp.sum(own_half * own_half, axis=1), 'tp')  5.08 us
  transfers between devices with their start and end apart: 2, of which 1 were waited for; matrix products, arithmetic and copies ran while one was open for 6% of the time, Pallas kernels for 0%

commit v1 on v0

v1 whole, which is shorter than its diff:
```python
import jax
import jax.numpy as jnp
from jax import lax
from jax.experimental import pallas as pl
from jax.experimental.pallas import tpu as pltpu
from jax.sharding import PartitionSpec as P

F32 = jnp.float32
BF16 = jnp.bfloat16
MESH = pl.DeviceIdType.MESH

EPS = 1e-06
LIMIT = 7.0
ALPHA = 1.702

SEQ = 64
HALF = 1024
STATES = 2048
CHAN = 512
PEERS = 64
SLOTS = 6
QUARTERS = 4
QW = HALF // QUARTERS
ROWS = SLOTS * QUARTERS
ALL = PEERS * ROWS
PAD = ALL + 8
GROUPS = 4
GP = PEERS // GROUPS
GROWS = GP * ROWS
GSLOTS = GP * SLOTS
BLK = 8 * ROWS
BSLOTS = 8 * SLOTS
ZSTEP = (0, 1, 3, 2)
CHUNKS = ((0, 1), (2, 3))

NT = (((1,), (1,)), ((), ()))


def mm(a, b):
    return jnp.dot(a, b, preferred_element_type=F32)


def mm_nt(a, b):
    return lax.dot_general(a, b, NT, preferred_element_type=F32)


def iota(shape, dim):
    return lax.broadcasted_iota(jnp.int32, shape, dim)


def div_small(v, d):
    return ((v.astype(F32) + 0.5) * (1.0 / d)).astype(jnp.int32)


def kernel(
    xg,
    ids_in,
    wts_in,
    state_in,
    mix_gain_in,
    in_proj_in,
    decay_in,
    freq_in,
    step_in,
    imap_in,
    omap_in,
    pscale_in,
    out_gain_in,
    out_proj_in,
    ffn_gain_in,
    wg_in,
    wu_in,
    wd_in,
    out_ref,
    nstate_ref,
    xv,
    ids,
    wts,
    state,
    mix_gain,
    in_proj,
    decay,
    freq,
    step,
    imap,
    omap,
    pscale,
    out_gain,
    out_proj,
    ffn_gain,
    wg,
    wu,
    wd,
    outv,
    nstate,
    actx,
    sqx,
    onehot,
    chi,
    clo,
    perm,
    permt,
    sendbuf,
    recv,
    rsend,
    rrecv,
    amat,
    hid,
    psend,
    prec,
    in_sems,
    out_sems,
    x_send,
    x_recv,
    d_send,
    d_recv,
    f_send,
    f_recv,
    p_send,
    p_recv,
    r_send,
    r_recv,
):
    ep = lax.axis_index("ep")
    tp = lax.axis_index("tp")
    other = 1 - tp
    z = lax.div(ep, 16)
    y = lax.rem(lax.div(ep, 4), 4)
    x = lax.rem(ep, 4)

    def peer_of(zstep, j, sign):
        dy = lax.div(j, 4)
        dx = lax.rem(j, 4)
        pz = lax.rem(z + sign * zstep + 4, 4)
        py = lax.rem(y + sign * dy + 4, 4)
        px = lax.rem(x + sign * dx + 4, 4)
        return pz * 16 + py * 4 + px

    barrier = pltpu.get_barrier_semaphore()
    pl.semaphore_signal(barrier, inc=1, device_id=(ep, other), device_id_type=MESH)
    for g in range(GROUPS):

        def greet(j, carry, g=g):
            pl.semaphore_signal(
                barrier, inc=1, device_id=(peer_of(ZSTEP[g], j, 1), tp), device_id_type=MESH
            )
            return carry

        lax.fori_loop(1 if g == 0 else 0, GP, greet, 0)

    pairs = (
        (xg, xv),
        (ids_in, ids),
        (wts_in, wts),
        (mix_gain_in, mix_gain),
        (in_proj_in, in_proj),
        (decay_in, decay),
        (freq_in, freq),
        (step_in, step),
        (imap_in, imap),
        (state_in, state),
        (omap_in, omap),
        (pscale_in, pscale),
        (out_gain_in, out_gain),
        (out_proj_in, out_proj),
        (ffn_gain_in, ffn_gain),
        (wg_in, wg),
        (wu_in, wu),
        (wd_in, wd),
    )
    loads = [pltpu.make_async_copy(a, b, in_sems.at[i]) for i, (a, b) in enumerate(pairs)]
    for load in loads:
        load.start()

    loads[1].wait()
    loads[2].wait()
    expert = iota((PEERS, SEQ), 0)
    named = jnp.zeros((PEERS, SEQ), F32)
    weight = jnp.zeros((PEERS, SEQ), F32)
    for k in range(4):
        hit = ids[k : k + 1, :] == expert
        named = named + jnp.where(hit, 1.0, 0.0)
        weight = weight + jnp.where(hit, wts[k : k + 1, :], 0.0)
    earlier = jnp.where(iota((SEQ, SEQ), 0) < iota((SEQ, SEQ), 1), 1.0, 0.0).astype(BF16)
    slot_of = named * (mm(named.astype(BF16), earlier) + 1.0)
    pos = iota((PEERS, PEERS), 0)
    gz = pos >> 4
    pz = (z + (gz ^ (gz >> 1))) & 3
    py = (y + ((pos >> 2) & 3)) & 3
    px = (x + (pos & 3)) & 3
    order = jnp.where(pz * 16 + py * 4 + px == iota((PEERS, PEERS), 1), 1.0, 0.0).astype(BF16)
    w_hi = weight.astype(BF16)
    w_lo = (weight - w_hi.astype(F32)).astype(BF16)
    slot_pt = mm(order, slot_of.astype(BF16)).astype(BF16)
    eye = jnp.where(iota((SEQ, SEQ), 0) == iota((SEQ, SEQ), 1), 1.0, 0.0).astype(BF16)

    def turned(v):
        return mm_nt(eye, v).astype(BF16)

    slot_tp = turned(slot_pt)
    whi_tp = turned(mm(order, w_hi).astype(BF16))
    wlo_tp = turned(mm(order, w_lo).astype(BF16))

    slot_p4 = jnp.concatenate([slot_pt] * QUARTERS, axis=1)
    row = iota((BLK, QUARTERS * SEQ), 0)
    rowp = div_small(row, ROWS)
    rem_row = row - rowp * ROWS
    rowq = div_small(rem_row, SLOTS)
    rows_ = rem_row - rowq * SLOTS
    want = jnp.where(rowq == (iota((BLK, QUARTERS * SEQ), 1) >> 6), rows_ + 1, -1).astype(F32)
    spread_row = div_small(iota((BLK, PEERS), 0), ROWS)
    spread_col = iota((BLK, PEERS), 1)
    for b in range(PEERS // 8):
        spread = jnp.where(spread_row + b * 8 == spread_col, 1.0, 0.0).astype(BF16)
        onehot[b * BLK : (b + 1) * BLK, :] = jnp.where(
            mm(spread, slot_p4) == want, 1.0, 0.0
        ).astype(BF16)

    def block_perm(rdim, cdim):
        r = iota((BLK, BLK), rdim)
        c = iota((BLK, BLK), cdim)
        rq = div_small(r, BSLOTS)
        rr = r - rq * BSLOTS
        rp = div_small(rr, SLOTS)
        rs = rr - rp * SLOTS
        return jnp.where(rp * ROWS + rq * SLOTS + rs == c, 1.0, 0.0).astype(BF16)

    perm[...] = block_perm(0, 1)
    permt[...] = block_perm(1, 0)

    loads[5].wait()
    loads[6].wait()
    loads[7].wait()
    rate_real = -decay[...]
    rate_imag = freq[...]
    n_groups, n_state = rate_real.shape
    diag = iota((n_groups, n_groups), 0) == iota((n_groups, n_groups), 1)
    time_step = jnp.sum(jnp.where(diag, step[...], 0.0), axis=1, keepdims=True)
    magnitude = jnp.exp(rate_real * time_step)
    phase = rate_imag * time_step
    bar_real = magnitude * jnp.cos(phase)
    bar_imag = magnitude * jnp.sin(phase)
    denominator = rate_real * rate_real + rate_imag * rate_imag
    shifted = bar_real - 1.0
    coef_real = (shifted * rate_real + bar_imag * rate_imag) / denominator
    coef_imag = (bar_imag * rate_real - shifted * rate_imag) / denominator
    own_group = iota((n_groups, STATES), 0) == (iota((n_groups, STATES), 1) >> 6)

    def as_row(v):
        wide = jnp.concatenate([v] * (STATES // n_state), axis=1)
        return jnp.sum(jnp.where(own_group, wide, 0.0), axis=0, keepdims=True)

    bar_real, bar_imag, coef_real, coef_imag = (
        as_row(v) for v in (bar_real, bar_imag, coef_real, coef_imag)
    )

    loads[0].wait()
    loads[3].wait()
    x0 = xv[0].astype(F32)
    x1 = xv[1].astype(F32)
    mean_sq = (
        jnp.sum(x0 * x0, axis=1, keepdims=True) + jnp.sum(x1 * x1, axis=1, keepdims=True)
    ) * (1.0 / (2 * HALF))
    scale = lax.rsqrt(mean_sq + EPS)
    n0 = (x0 * scale * mix_gain[:, :HALF]).astype(BF16)
    n1 = (x1 * scale * mix_gain[:, HALF:]).astype(BF16)
    loads[4].wait()
    channels = (mm(n0, in_proj[:HALF, :]) + mm(n1, in_proj[HALF:, :])).astype(BF16)
    loads[8].wait()
    loads[9].wait()
    loads[10].wait()
    loads[11].wait()
    same = (iota((128, 512), 0) >> 4) == (iota((128, 512), 1) >> 6)

    def spread_groups(m):
        return jnp.where(same, jnp.concatenate([m] * 8, axis=1), 0.0).astype(BF16)

    for b in range(4):
        rows = slice(b * 128, (b + 1) * 128)
        cols = slice(b * 512, (b + 1) * 512)
        ch = channels[:, rows]
        u0 = mm(ch, spread_groups(imap[0, rows, :]))
        u1 = mm(ch, spread_groups(imap[1, rows, :]))
        hr = state[0, :, cols]
        hi = state[1, :, cols]
        br, bi = bar_real[:, cols], bar_imag[:, cols]
        cr, ci = coef_real[:, cols], coef_imag[:, cols]
        nr = br * hr - bi * hi + (cr * u0 - ci * u1)
        ni = br * hi + bi * hr + (cr * u1 + ci * u0)
        nstate[0, :, cols] = nr
        nstate[1, :, cols] = ni
        mixed = (
            mm_nt(nr.astype(BF16), spread_groups(omap[0, rows, :]))
            - mm_nt(ni.astype(BF16), spread_groups(omap[1, rows, :]))
            + pscale[:, rows] * ch.astype(F32)
        )
        actx[tp, :, rows] = jax.nn.gelu(mixed, approximate=True).astype(BF16)
    store_state = pltpu.make_async_copy(nstate, nstate_ref, out_sems.at[0])
    store_state.start()

    pl.semaphore_wait(barrier, PEERS)

    def to_partner(ref, send, recv_):
        return pltpu.make_async_remote_copy(
            src_ref=ref, dst_ref=ref, send_sem=send, recv_sem=recv_,
            device_id=(ep, other), device_id_type=MESH,
        )

    act_copy = to_partner(actx.at[tp], x_send.at[0], x_recv.at[0])
    act_copy.start()
    loads[12].wait()
    loads[13].wait()
    loads[14].wait()
    act_copy.wait()
    a0 = actx[0].astype(F32)
    a1 = actx[1].astype(F32)
    mean_sq = (
        jnp.sum(a0 * a0, axis=1, keepdims=True) + jnp.sum(a1 * a1, axis=1, keepdims=True)
    ) * (1.0 / (2 * CHAN))
    scale = lax.rsqrt(mean_sq + EPS)
    s0 = (a0 * scale * out_gain[:, :CHAN]).astype(BF16)
    s1 = (a1 * scale * out_gain[:, CHAN:]).astype(BF16)
    after = (
        xv[tp].astype(F32) + (mm(s0, out_proj[:CHAN, :]) + mm(s1, out_proj[CHAN:, :]))
    ).astype(BF16)
    outv[...] = after
    after32 = after.astype(F32)
    sqx[tp] = jnp.broadcast_to(jnp.sum(after32 * after32, axis=1, keepdims=True), (SEQ, 128))
    sq_copy = to_partner(sqx.at[tp], x_send.at[1], x_recv.at[1])
    sq_copy.start()
    sq_copy.wait()
    mean_sq = (sqx[0] + sqx[1])[:, :1] * (1.0 / (2 * HALF))
    expert_in = (after32 * lax.rsqrt(mean_sq + EPS) * ffn_gain[tp]).astype(BF16)
    stacked = jnp.concatenate(
        [expert_in[:, q * QW : (q + 1) * QW] for q in range(QUARTERS)], axis=0
    )

    def block_at(ref, p):
        return ref.at[pl.ds(pl.multiple_of(p * ROWS, 8), ROWS)]

    for g in range(GROUPS):
        rows = slice(g * GROWS, (g + 1) * GROWS)
        sendbuf[rows, :] = mm(onehot[rows, :], stacked).astype(BF16)

        def dispatch(j, carry, g=g):
            p = g * GP + j
            pltpu.make_async_remote_copy(
                src_ref=block_at(sendbuf, p), dst_ref=block_at(recv.at[tp], p),
                send_sem=d_send, recv_sem=d_recv.at[g],
                device_id=(peer_of(ZSTEP[g], j, 1), tp), device_id_type=MESH,
            ).start()
            return carry

        lax.fori_loop(1 if g == 0 else 0, GP, dispatch, 0)
    recv[tp, :ROWS, :] = sendbuf[:ROWS, :]

    col = iota((PEERS, ALL), 1)
    spread_t = jnp.where(div_small(col, ROWS) == iota((PEERS, ALL), 0), 1.0, 0.0).astype(BF16)
    c1 = iota((1, ALL), 1)
    c1 = c1 - div_small(c1, ROWS) * ROWS
    cq = div_small(c1, SLOTS)
    cs = (c1 - cq * SLOTS + 1).astype(F32)
    slot_x = mm(slot_tp, spread_t)
    whi_x = mm(whi_tp, spread_t)
    wlo_x = mm(wlo_tp, spread_t)
    hit = slot_x == cs
    for q in range(QUARTERS):
        keep = hit & (cq == q)
        chi[q * SEQ : (q + 1) * SEQ, :] = jnp.where(keep, whi_x, 0.0).astype(BF16)
        clo[q * SEQ : (q + 1) * SEQ, :] = jnp.where(keep, wlo_x, 0.0).astype(BF16)

    loads[15].wait()
    loads[16].wait()
    loads[17].wait()

    def arrived(ref, sem):
        pltpu.make_async_remote_copy(
            src_ref=ref, dst_ref=ref, send_sem=sem, recv_sem=sem,
            device_id=(ep, other), device_id_type=MESH,
        ).wait_recv()

    def group_rows(g):
        first = g * GROWS
        return (first + ROWS, GROWS - ROWS) if g == 0 else (first, GROWS)

    def forward(g):
        first, count = group_rows(g)
        arrived(recv.at[tp, pl.ds(first, count)], d_recv.at[g])
        copy = to_partner(
            recv.at[tp, pl.ds(g * GROWS, GROWS)], f_send.at[g], f_recv.at[g]
        )
        copy.start()
        return copy

    started = []
    for c, chunk in enumerate(CHUNKS):
        copies = [forward(g) for g in chunk]
        started += copies
        first_slot = chunk[0] * GSLOTS
        slots = len(chunk) * GSLOTS
        for copy in copies:
            copy.wait_recv()
        for b in range(len(chunk) * 2):
            r0 = chunk[0] * GROWS + b * BLK
            s0_ = first_slot + b * BSLOTS
            for h in range(2):
                moved = mm(perm[...], recv[h, r0 : r0 + BLK, :]).astype(BF16)
                for q in range(QUARTERS):
                    amat[s0_ : s0_ + BSLOTS, h * HALF + q * QW : h * HALF + (q + 1) * QW] = moved[
                        q * BSLOTS : (q + 1) * BSLOTS, :
                    ]
        srows = slice(first_slot, first_slot + slots)

        def units(n, carry):
            at = pl.ds(pl.multiple_of(n * 256, 256), 256)
            gate = mm(amat[srows, :], wg[:, at])
            up = mm(amat[srows, :], wu[:, at])
            gated = jnp.minimum(gate, LIMIT)
            act = (jnp.clip(up, -LIMIT, LIMIT) + 1.0) * gated * jax.nn.sigmoid(ALPHA * gated)
            hid[srows, at] = act.astype(BF16)
            return carry

        lax.fori_loop(0, 4, units, 0)

        def down_other(n, carry):
            at = pl.ds(pl.multiple_of(n * 256, 256), 256)
            wat = pl.ds(pl.multiple_of(other * HALF + n * 256, 256), 256)
            psend[srows, at] = mm(hid[srows, :], wd[:, wat]).astype(BF16)
            return carry

        lax.fori_loop(0, 4, down_other, 0)
        part_copy = pltpu.make_async_remote_copy(
            src_ref=psend.at[srows], dst_ref=prec.at[srows],
            send_sem=p_send.at[c], recv_sem=p_recv.at[c],
            device_id=(ep, other), device_id_type=MESH,
        )
        part_copy.start()
        started.append(part_copy)

        def down_own(n, carry):
            at = pl.ds(pl.multiple_of(n * 256, 256), 256)
            wat = pl.ds(pl.multiple_of(tp * HALF + n * 256, 256), 256)
            amat[srows, at] = mm(hid[srows, :], wd[:, wat]).astype(BF16)
            return carry

        lax.fori_loop(0, 4, down_own, 0)
        part_copy.wait_recv()
        for i, g in enumerate(chunk):
            for b in range(2):
                s0_ = first_slot + (2 * i + b) * BSLOTS
                total = (
                    amat[s0_ : s0_ + BSLOTS, :HALF].astype(F32)
                    + prec[s0_ : s0_ + BSLOTS, :].astype(F32)
                ).astype(BF16)
                tall = jnp.concatenate(
                    [total[:, q * QW : (q + 1) * QW] for q in range(QUARTERS)], axis=0
                )
                r0 = g * GROWS + b * BLK
                rsend[r0 : r0 + BLK, :] = mm(permt[...], tall).astype(BF16)

            def give_back(j, carry, g=g):
                p = g * GP + j
                pltpu.make_async_remote_copy(
                    src_ref=block_at(rsend, p), dst_ref=block_at(rrecv, p),
                    send_sem=r_send, recv_sem=r_recv.at[g],
                    device_id=(peer_of(ZSTEP[g], j, -1), tp), device_id_type=MESH,
                ).start()
                return carry

            lax.fori_loop(1 if g == 0 else 0, GP, give_back, 0)
            if g == 0:
                rrecv[:ROWS, :] = rsend[:ROWS, :]

    total = jnp.zeros((QUARTERS * SEQ, QW), F32)
    for g in range(GROUPS):
        first, count = group_rows(g)
        arrived(rrecv.at[pl.ds(first, count)], r_recv.at[g])
        rows = slice(g * GROWS, (g + 1) * GROWS)
        got = rrecv[rows, :]
        total = total + mm(chi[:, rows], got) + mm(clo[:, rows], got)
    for q in range(QUARTERS):
        cols = slice(q * QW, (q + 1) * QW)
        outv[:, cols] = (
            outv[:, cols].astype(F32) + total[q * SEQ : (q + 1) * SEQ, :]
        ).astype(BF16)
    store_out = pltpu.make_async_copy(outv, out_ref, out_sems.at[1])
    store_out.start()

    for copy in started:
        copy.wait_send()
    for sem, buf in ((d_send, sendbuf), (r_send, rsend)):
        sent = buf.at[pl.ds(ROWS, ALL - ROWS)]
        pltpu.make_async_remote_copy(
            src_ref=sent, dst_ref=sent, send_sem=sem, recv_sem=sem,
            device_id=(ep, other), device_id_type=MESH,
        ).wait_send()
    store_state.wait()
    store_out.wait()


def local(
    residual,
    route_ids,
    route_weights,
    carried_state,
    mix_gain,
    in_proj,
    decay_rate,
    frequency,
    step_size,
    input_map,
    output_matrix,
    passthrough_scale,
    out_gain,
    out_proj,
    ffn_gain,
    w_gate,
    w_up,
    w_down,
):
    xg = lax.all_gather(residual, "tp", axis=0)
    args = (
        xg,
        route_ids.T,
        route_weights.T,
        carried_state,
        mix_gain.reshape(1, -1),
        in_proj,
        decay_rate,
        frequency,
        step_size.reshape(1, -1),
        jnp.swapaxes(input_map, 2, 3).reshape(2, CHAN, -1),
        output_matrix.reshape(2, CHAN, -1),
        passthrough_scale.reshape(1, -1),
        out_gain.reshape(1, -1),
        out_proj,
        ffn_gain.reshape(2, 1, -1),
        w_gate.reshape(w_gate.shape[1:]),
        w_up.reshape(w_up.shape[1:]),
        w_down.reshape(w_down.shape[1:]),
    )
    dma = pltpu.SemaphoreType.DMA
    vmem = pltpu.VMEM
    updated, new_state = pl.pallas_call(
        kernel,
        out_shape=(
            jax.ShapeDtypeStruct(residual.shape, BF16),
            jax.ShapeDtypeStruct(carried_state.shape, F32),
        ),
        in_specs=[pl.BlockSpec(memory_space=pl.ANY)] * len(args),
        out_specs=(pl.BlockSpec(memory_space=pl.ANY),) * 2,
        scratch_shapes=[vmem(a.shape, a.dtype) for a in args]
        + [
            vmem((SEQ, HALF), BF16),
            vmem(carried_state.shape, F32),
            vmem((2, SEQ, CHAN), BF16),
            vmem((2, SEQ, 128), F32),
            vmem((ALL, QUARTERS * SEQ), BF16),
            vmem((QUARTERS * SEQ, ALL), BF16),
            vmem((QUARTERS * SEQ, ALL), BF16),
            vmem((BLK, BLK), BF16),
            vmem((BLK, BLK), BF16),
            vmem((PAD, QW), BF16),
            vmem((2, PAD, QW), BF16),
            vmem((PAD, QW), BF16),
            vmem((PAD, QW), BF16),
            vmem((PEERS * SLOTS, 2 * HALF), BF16),
            vmem((PEERS * SLOTS, HALF), BF16),
            vmem((PEERS * SLOTS, HALF), BF16),
            vmem((PEERS * SLOTS, HALF), BF16),
            dma((len(args),)),
            dma((2,)),
            dma((2,)),
            dma((2,)),
            dma,
            dma((GROUPS,)),
            dma((GROUPS,)),
            dma((GROUPS,)),
            dma((len(CHUNKS),)),
            dma((len(CHUNKS),)),
            dma,
            dma((GROUPS,)),
        ],
        compiler_params=pltpu.CompilerParams(
            collective_id=0, has_side_effects=True, vmem_limit_bytes=60 * 1024 * 1024
        ),
    )(*args)
    return updated, new_state


def solution(mesh):
    placed = (
        P("ep", "tp"),
        P("ep", None),
        P("ep", None),
        P(None, "ep", "tp"),
        P(),
        P(None, "tp"),
        P("tp", None),
        P("tp", None),
        P("tp"),
        P(None, "tp", None, None),
        P(None, "tp", None, None),
        P("tp"),
        P(),
        P(None, "tp"),
        P(),
        P("ep", None, "tp"),
        P("ep", None, "tp"),
        P("ep", "tp", None),
    )
    return jax.shard_map(
        local,
        mesh=mesh,
        in_specs=placed,
        out_specs=(P("ep", "tp"), P(None, "ep", "tp")),
        check_vma=False,
    )
```

time: 134 us -> 57.2 us (0.43)
  Pallas kernels: 0 us -> 47.7 us
  blocking collectives: 49.8 us -> 4.77 us
  matrix products: 26.4 us -> 0 us
  local copies, waits for them, and re-layouts: 28 us -> 3.86 us
  waiting for transfers between devices: 12 us -> 0 us
  starting transfers between devices: 9.35 us -> 0 us
  other arithmetic: 6.82 us -> 0 us
    pallas_call x0 -> x1, Pallas kernels: none -> 47.7 us  [local(): pl.pallas_call(kernel, out_shape=(jax.ShapeDtypeStruct(residual.shape, BF...]
    all_to_all x3 -> x0, blocking collectives: 41.3 us -> none  [the longest x1 29.2 us: local(): lax.all_to_all(buffer, 'ep', split_axis=0, concat_axis=0, tiled=True)]
    dot_general x9 -> x0, matrix products: 26.4 us -> none  [the longest x1 9.23 us: local(): jnp.einsum('necf,efd->necd', activation, w_down, preferred_element_type=j...]
    all_to_all x2 -> x0, waiting for transfers between devices: 12 us -> none  [the longest x1 12 us: local(): lax.all_to_all(summed, 'ep', split_axis=0, concat_axis=0, tiled=True)]
    all_to_all x2 -> x0, starting transfers between devices: 9.35 us -> none  [the longest x1 5.64 us: local(): lax.all_to_all(summed, 'ep', split_axis=0, concat_axis=0, tiled=True)]
    another operation x4 -> x0, local copies, waits for them, and re-layouts: 7.34 us -> none
    psum x2 -> x0, blocking collectives: 5.08 us -> none  [local(): total_sq = lax.psum(jnp.sum(own_half * own_half, axis=1), 'tp')]
    slice x4 -> x0, local copies, waits for them, and re-layouts: 4.97 us -> none  [the longest x2 2.43 us: state_step(): carried_state[0].reshape(row_count, number_of_groups, state_width)]
  transfers between devices with their start and end apart: 2 -> 0, of which waited for: 1 -> 0; matrix products, arithmetic and copies ran while one was open for 6% -> 0% of each run, Pallas kernels for 0% -> 0%
where the time goes in v1:
time: 57.2 us; the launch traced here: 57 us
  Pallas kernels  47.7 us (83%)
  blocking collectives  4.77 us (8%)
  local copies, waits for them, and re-layouts  3.86 us (7%)
  between operations  0.64 us (1%)
    pallas_call x1, Pallas kernels, local(): pl.pallas_call(kernel, out_shape=(jax.ShapeDtypeStruct(residual.shape, BF...  47.7 us
    all_gather x1, blocking collectives, local(): xg = lax.all_gather(residual, 'tp', axis=0)  4.77 us
    unnamed x2, local copies, waits for them, and re-layouts  3.86 us

profile of v1, /device:TPU:1, one launch (start us, length us, event | category | flops | bytes accessed | tf_op | source)
XLA Modules:
  0.0 57.0 jit_solution(5557605970101028860)
XLA Ops:
  0.6 4.8 %all-gather = bf16[128,1024]{1,0:T(8,128)(2,1)} all-gather(bf16[64,1024]{1,0:T(8,128)(2,1)} %param.18), channel_id=2, replica_groups=mesh['ep'=64,'tp'=2] {'tp'}, dimensions={0}, use_global_device_ids=true | all-gather | bytes 393216 | tf_op jit(solution)/shard_map/all_gather | solution.py:521
  5.4 47.7 %shard_map.185 = (bf16[64,1024]{1,0:T(8,128)(2,1)}, f32[2,64,2048]{2,1,0:T(8,128)}) custom-call(bf16[2,64,1024]{2,1,0:T(8,128)(2,1)} %bitcast.18, s32[4,64]{1,0:T(4,128)} %bitcast.24, f32[4,64]{1,0:T(4,128)} %bitcast.25, f32[2,64,2048]{2,1,0:T(8,128)} %state_in.1, f32[1,2048]{1,0:T(1,128)} %bitcast.21, bf16[2048,512]{1,0:T(8,128)(2,1)} %in_proj_in.1, ...), custom_call_target="tpu_custom_call" | custom-call | tf_op jit(solution)/shard_map/pallas_call | solution.py:544
  53.1 1.6 %copy.22 = bf16[64,1024]{1,0:T(8,128)(2,1)} copy(bf16[64,1024]{1,0:T(8,128)(2,1)} %get-tuple-element.4) | data formatting | bytes 262144
  54.7 2.3 %copy.23 = f32[2,64,2048]{2,1,0:T(8,128)} copy(f32[2,64,2048]{2,1,0:T(8,128)} %get-tuple-element.5) | data formatting | bytes 2097152

commit v2 on v1

v2 whole, which is shorter than its diff:
```python
import jax
import jax.numpy as jnp
from jax import lax
from jax.experimental import pallas as pl
from jax.experimental.pallas import tpu as pltpu
from jax.sharding import PartitionSpec as P

F32 = jnp.float32
BF16 = jnp.bfloat16
MESH = pl.DeviceIdType.MESH

VMEM_LIMIT = 62 * 1024 * 1024
EPS = 1e-06
LIMIT = 7.0
ALPHA = 1.702

SEQ = 64
HALF = 1024
STATES = 2048
CHAN = 512
PEERS = 64
SLOTS = 6
QUARTERS = 4
QW = HALF // QUARTERS
ROWS = SLOTS * QUARTERS
ALL = PEERS * ROWS
PAD = ALL + 8
OWN = ALL - ROWS
GROUPS = 8
GP = PEERS // GROUPS
GROWS = GP * ROWS
GSLOTS = GP * SLOTS
CHUNKS = ((0, 1, 2), (3, 4, 5), (6, 7))


def hops(step):
    return sum(min(d, 4 - d) for d in step)


STEPS = sorted(
    ((dz, dy, dx) for dz in range(4) for dy in range(4) for dx in range(4)), key=hops, reverse=True
)

NT = (((1,), (1,)), ((), ()))


def mm(a, b):
    return jnp.dot(a, b, preferred_element_type=F32)


def mm_nt(a, b):
    return lax.dot_general(a, b, NT, preferred_element_type=F32)


def iota(shape, dim):
    return lax.broadcasted_iota(jnp.int32, shape, dim)


def div_small(v, d):
    return ((v.astype(F32) + 0.5) * (1.0 / d)).astype(jnp.int32)


def kernel(
    x_in,
    ids_in,
    wts_in,
    decay_in,
    freq_in,
    step_in,
    imap_in,
    omap_in,
    mix_gain_in,
    in_proj_in,
    state_in,
    pscale_in,
    out_gain_in,
    out_proj_in,
    ffn_gain_in,
    wg_in,
    wu_in,
    wd_in,
    out_ref,
    nstate_ref,
    outv,
    nstate,
    xv,
    ids,
    wts,
    decay,
    freq,
    step,
    imap,
    omap,
    mix_gain,
    in_proj,
    state,
    pscale,
    out_gain,
    out_proj,
    ffn_gain,
    wg,
    wu,
    wd,
    inmix,
    outmix,
    actx,
    sqx,
    onehot,
    chi,
    clo,
    perm,
    permt,
    sendbuf,
    recv,
    rsend,
    rrecv,
    amat,
    hid,
    psend,
    prec,
    in_sems,
    out_sems,
    x_send,
    x_recv,
    d_send,
    d_recv,
    f_send,
    f_recv,
    p_send,
    p_recv,
    r_send,
    r_recv,
):
    ep = lax.axis_index("ep")
    tp = lax.axis_index("tp")
    other = 1 - tp
    z = lax.div(ep, 16)
    y = lax.rem(lax.div(ep, 4), 4)
    x = lax.rem(ep, 4)
    z_at = [lax.rem(z + d, 4) * 16 for d in range(4)]
    y_at = [lax.rem(y + d, 4) * 4 for d in range(4)]
    x_at = [lax.rem(x + d, 4) for d in range(4)]

    def peer_of(p, sign):
        dz, dy, dx = STEPS[p]
        return z_at[sign * dz % 4] + y_at[sign * dy % 4] + x_at[sign * dx % 4]

    barrier = pltpu.get_barrier_semaphore()
    pl.semaphore_signal(barrier, inc=1, device_id=(ep, other), device_id_type=MESH)

    def greet(i, carry):
        pl.semaphore_signal(
            barrier, inc=1, device_id=(lax.rem(ep + i, PEERS), tp), device_id_type=MESH
        )
        return carry

    lax.fori_loop(1, PEERS, greet, 0)

    pairs = (
        (x_in, xv.at[tp]),
        (ids_in, ids),
        (wts_in, wts),
        (decay_in, decay),
        (freq_in, freq),
        (step_in, step),
        (imap_in, imap),
        (omap_in, omap),
        (mix_gain_in, mix_gain),
        (in_proj_in, in_proj),
        (state_in, state),
        (pscale_in, pscale),
        (out_gain_in, out_gain),
        (out_proj_in, out_proj),
        (ffn_gain_in, ffn_gain),
        (wg_in, wg),
        (wu_in, wu),
        (wd_in, wd),
    )
    loads = [pltpu.make_async_copy(a, b, in_sems.at[i]) for i, (a, b) in enumerate(pairs)]
    for load in loads:
        load.start()

    loads[1].wait()
    loads[2].wait()
    expert = iota((PEERS, SEQ), 0)
    named = jnp.zeros((PEERS, SEQ), F32)
    weight = jnp.zeros((PEERS, SEQ), F32)
    for k in range(4):
        hit = ids[k : k + 1, :] == expert
        named = named + jnp.where(hit, 1.0, 0.0)
        weight = weight + jnp.where(hit, wts[k : k + 1, :], 0.0)
    earlier = jnp.where(iota((SEQ, SEQ), 0) < iota((SEQ, SEQ), 1), 1.0, 0.0).astype(BF16)
    slot_of = named * (mm(named.astype(BF16), earlier) + 1.0)
    pos = iota((PEERS, PEERS), 0)
    named_at = jnp.zeros((PEERS, PEERS), jnp.int32)
    for p in range(PEERS):
        named_at = jnp.where(pos == p, peer_of(p, 1), named_at)
    order = jnp.where(named_at == iota((PEERS, PEERS), 1), 1.0, 0.0).astype(BF16)
    w_hi = weight.astype(BF16)
    w_lo = (weight - w_hi.astype(F32)).astype(BF16)
    slot_pt = mm(order, slot_of.astype(BF16)).astype(BF16)
    eye = jnp.where(iota((SEQ, SEQ), 0) == iota((SEQ, SEQ), 1), 1.0, 0.0).astype(BF16)

    def turned(v):
        return mm_nt(eye, v).astype(BF16)

    slot_tp = turned(slot_pt)
    whi_tp = turned(mm(order, w_hi).astype(BF16))
    wlo_tp = turned(mm(order, w_lo).astype(BF16))

    slot_p4 = jnp.concatenate([slot_pt] * QUARTERS, axis=1)
    row = iota((GROWS, QUARTERS * SEQ), 0)
    rowp = div_small(row, ROWS)
    rem_row = row - rowp * ROWS
    rowq = div_small(rem_row, SLOTS)
    rows_ = rem_row - rowq * SLOTS
    want = jnp.where(rowq == (iota((GROWS, QUARTERS * SEQ), 1) >> 6), rows_ + 1, -1).astype(F32)
    spread_row = div_small(iota((GROWS, PEERS), 0), ROWS)
    spread_col = iota((GROWS, PEERS), 1)
    for b in range(GROUPS):
        spread = jnp.where(spread_row + b * 8 == spread_col, 1.0, 0.0).astype(BF16)
        onehot[b * GROWS : (b + 1) * GROWS, :] = jnp.where(
            mm(spread, slot_p4) == want, 1.0, 0.0
        ).astype(BF16)

    def block_perm(rdim, cdim):
        r = iota((GROWS, GROWS), rdim)
        c = iota((GROWS, GROWS), cdim)
        rq = div_small(r, GSLOTS)
        rr = r - rq * GSLOTS
        rp = div_small(rr, SLOTS)
        rs = rr - rp * SLOTS
        return jnp.where(rp * ROWS + rq * SLOTS + rs == c, 1.0, 0.0).astype(BF16)

    perm[...] = block_perm(0, 1)
    permt[...] = block_perm(1, 0)

    loads[3].wait()
    loads[4].wait()
    loads[5].wait()
    rate_real = -decay[...]
    rate_imag = freq[...]
    n_groups, n_state = rate_real.shape
    diag = iota((n_groups, n_groups), 0) == iota((n_groups, n_groups), 1)
    time_step = jnp.sum(jnp.where(diag, step[...], 0.0), axis=1, keepdims=True)
    magnitude = jnp.exp(rate_real * time_step)
    phase = rate_imag * time_step
    bar_real = magnitude * jnp.cos(phase)
    bar_imag = magnitude * jnp.sin(phase)
    denominator = rate_real * rate_real + rate_imag * rate_imag
    shifted = bar_real - 1.0
    coef_real = (shifted * rate_real + bar_imag * rate_imag) / denominator
    coef_imag = (bar_imag * rate_real - shifted * rate_imag) / denominator
    own_group = iota((n_groups, STATES), 0) == (iota((n_groups, STATES), 1) >> 6)

    def as_row(v):
        wide = jnp.concatenate([v] * (STATES // n_state), axis=1)
        return jnp.sum(jnp.where(own_group, wide, 0.0), axis=0, keepdims=True)

    bar_real, bar_imag, coef_real, coef_imag = (
        as_row(v) for v in (bar_real, bar_imag, coef_real, coef_imag)
    )

    same = (iota((128, 512), 0) >> 4) == (iota((128, 512), 1) >> 6)

    def spread_groups(m):
        return jnp.where(same, jnp.concatenate([m] * 8, axis=1), 0.0).astype(BF16)

    loads[6].wait()
    loads[7].wait()
    for b in range(4):
        rows = slice(b * 128, (b + 1) * 128)
        for i in range(2):
            inmix[i, rows, :] = spread_groups(imap[i, rows, :])
        outmix[0, rows, :] = spread_groups(omap[0, rows, :])
        outmix[1, rows, :] = spread_groups(-omap[1, rows, :])

    loads[0].wait()
    pl.semaphore_wait(barrier, PEERS)

    def to_partner(ref, send, recv_):
        return pltpu.make_async_remote_copy(
            src_ref=ref, dst_ref=ref, send_sem=send, recv_sem=recv_,
            device_id=(ep, other), device_id_type=MESH,
        )

    x_copy = to_partner(xv.at[tp], x_send.at[2], x_recv.at[2])
    x_copy.start()
    loads[10].wait()
    for b in range(4):
        cols = slice(b * 512, (b + 1) * 512)
        hr = state[0, :, cols]
        hi = state[1, :, cols]
        br, bi = bar_real[:, cols], bar_imag[:, cols]
        nstate[0, :, cols] = br * hr - bi * hi
        nstate[1, :, cols] = br * hi + bi * hr
    loads[8].wait()
    loads[9].wait()
    loads[11].wait()
    x_copy.wait()
    x0 = xv[0].astype(F32)
    x1 = xv[1].astype(F32)
    mean_sq = (
        jnp.sum(x0 * x0, axis=1, keepdims=True) + jnp.sum(x1 * x1, axis=1, keepdims=True)
    ) * (1.0 / (2 * HALF))
    scale = lax.rsqrt(mean_sq + EPS)
    n0 = (x0 * scale * mix_gain[:, :HALF]).astype(BF16)
    n1 = (x1 * scale * mix_gain[:, HALF:]).astype(BF16)
    channels = (mm(n0, in_proj[:HALF, :]) + mm(n1, in_proj[HALF:, :])).astype(BF16)
    for b in range(4):
        rows = slice(b * 128, (b + 1) * 128)
        cols = slice(b * 512, (b + 1) * 512)
        ch = channels[:, rows]
        u0 = mm(ch, inmix[0, rows, :])
        u1 = mm(ch, inmix[1, rows, :])
        cr, ci = coef_real[:, cols], coef_imag[:, cols]
        nr = nstate[0, :, cols] + (cr * u0 - ci * u1)
        ni = nstate[1, :, cols] + (cr * u1 + ci * u0)
        nstate[0, :, cols] = nr
        nstate[1, :, cols] = ni
        mixed = (
            mm_nt(nr.astype(BF16), outmix[0, rows, :])
            + mm_nt(ni.astype(BF16), outmix[1, rows, :])
            + pscale[:, rows] * ch.astype(F32)
        )
        actx[tp, :, rows] = jax.nn.gelu(mixed, approximate=True).astype(BF16)

    store_state = pltpu.make_async_copy(nstate, nstate_ref, out_sems.at[0])
    store_state.start()
    act_copy = to_partner(actx.at[tp], x_send.at[0], x_recv.at[0])
    act_copy.start()
    loads[12].wait()
    loads[13].wait()
    loads[14].wait()
    act_copy.wait()
    a0 = actx[0].astype(F32)
    a1 = actx[1].astype(F32)
    mean_sq = (
        jnp.sum(a0 * a0, axis=1, keepdims=True) + jnp.sum(a1 * a1, axis=1, keepdims=True)
    ) * (1.0 / (2 * CHAN))
    scale = lax.rsqrt(mean_sq + EPS)
    s0 = (a0 * scale * out_gain[:, :CHAN]).astype(BF16)
    s1 = (a1 * scale * out_gain[:, CHAN:]).astype(BF16)
    after = (
        xv[tp].astype(F32) + (mm(s0, out_proj[:CHAN, :]) + mm(s1, out_proj[CHAN:, :]))
    ).astype(BF16)
    outv[...] = after
    after32 = after.astype(F32)
    sqx[tp] = jnp.broadcast_to(jnp.sum(after32 * after32, axis=1, keepdims=True), (SEQ, 128))
    sq_copy = to_partner(sqx.at[tp], x_send.at[1], x_recv.at[1])
    sq_copy.start()
    sq_copy.wait()
    mean_sq = (sqx[0] + sqx[1])[:, :1] * (1.0 / (2 * HALF))
    expert_in = (after32 * lax.rsqrt(mean_sq + EPS) * ffn_gain[tp]).astype(BF16)
    stacked = jnp.concatenate(
        [expert_in[:, q * QW : (q + 1) * QW] for q in range(QUARTERS)], axis=0
    )

    def send_block(src, dst, p, sign, send, recv_):
        at = pl.ds(p * ROWS, ROWS)
        pltpu.make_async_remote_copy(
            src_ref=src.at[at], dst_ref=dst.at[at], send_sem=send, recv_sem=recv_,
            device_id=(peer_of(p, sign), tp), device_id_type=MESH,
        ).start()

    for b in range(4):
        rows = slice(b * 2 * GROWS, (b + 1) * 2 * GROWS)
        sendbuf[rows, :] = mm(onehot[rows, :], stacked).astype(BF16)
        for p in range(b * 2 * GP, min((b + 1) * 2 * GP, PEERS - 1)):
            send_block(sendbuf, recv.at[tp], p, 1, d_send, d_recv.at[p // GP])
    recv[tp, OWN:ALL, :] = sendbuf[OWN:ALL, :]

    col = iota((PEERS, ALL), 1)
    spread_t = jnp.where(div_small(col, ROWS) == iota((PEERS, ALL), 0), 1.0, 0.0).astype(BF16)
    c1 = iota((1, ALL), 1)
    c1 = c1 - div_small(c1, ROWS) * ROWS
    cq = div_small(c1, SLOTS)
    cs = (c1 - cq * SLOTS + 1).astype(F32)
    slot_x = mm(slot_tp, spread_t)
    whi_x = mm(whi_tp, spread_t)
    wlo_x = mm(wlo_tp, spread_t)
    hit = slot_x == cs
    for q in range(QUARTERS):
        keep = hit & (cq == q)
        chi[q * SEQ : (q + 1) * SEQ, :] = jnp.where(keep, whi_x, 0.0).astype(BF16)
        clo[q * SEQ : (q + 1) * SEQ, :] = jnp.where(keep, wlo_x, 0.0).astype(BF16)

    loads[15].wait()
    loads[16].wait()
    loads[17].wait()

    def arrived(ref, sem):
        pltpu.make_async_remote_copy(
            src_ref=ref, dst_ref=ref, send_sem=sem, recv_sem=sem,
            device_id=(ep, other), device_id_type=MESH,
        ).wait_recv()

    started = []
    forwards = [None] * GROUPS

    def forward(g):
        first = g * GROWS
        count = min(GROWS, OWN - first)
        arrived(recv.at[tp, pl.ds(first, count)], d_recv.at[g])
        copy = to_partner(recv.at[tp, pl.ds(first, GROWS)], f_send.at[g], f_recv.at[g])
        copy.start()
        started.append(copy)
        forwards[g] = copy

    def assemble(g):
        forwards[g].wait_recv()
        slots = slice(g * GSLOTS, (g + 1) * GSLOTS)
        for h in range(2):
            moved = mm(perm[...], recv[h, g * GROWS : (g + 1) * GROWS, :]).astype(BF16)
            for q in range(QUARTERS):
                amat[slots, h * HALF + q * QW : h * HALF + (q + 1) * QW] = moved[
                    q * GSLOTS : (q + 1) * GSLOTS, :
                ]

    for g in CHUNKS[0]:
        forward(g)
    for g in CHUNKS[0]:
        assemble(g)
    for c, chunk in enumerate(CHUNKS):
        following = CHUNKS[c + 1] if c + 1 < len(CHUNKS) else ()
        srows = slice(chunk[0] * GSLOTS, (chunk[-1] + 1) * GSLOTS)
        lhs = amat[srows, :]
        for n in range(2):
            at = slice(n * 512, (n + 1) * 512)
            gate = mm(lhs, wg[:, at])
            up = mm(lhs, wu[:, at])
            gated = jnp.minimum(gate, LIMIT)
            act = (jnp.clip(up, -LIMIT, LIMIT) + 1.0) * gated * jax.nn.sigmoid(ALPHA * gated)
            hid[srows, at] = act.astype(BF16)
        for g in following:
            forward(g)
        lhs = hid[srows, :]
        for n in range(2):
            wat = pl.ds(pl.multiple_of(other * HALF + n * 512, 512), 512)
            psend[srows, n * 512 : (n + 1) * 512] = mm(lhs, wd[:, wat]).astype(BF16)
        part_copy = pltpu.make_async_remote_copy(
            src_ref=psend.at[srows], dst_ref=prec.at[srows],
            send_sem=p_send.at[c], recv_sem=p_recv.at[c],
            device_id=(ep, other), device_id_type=MESH,
        )
        part_copy.start()
        started.append(part_copy)
        for n in range(2):
            wat = pl.ds(pl.multiple_of(tp * HALF + n * 512, 512), 512)
            amat[srows, n * 512 : (n + 1) * 512] = mm(lhs, wd[:, wat]).astype(BF16)
        for g in following:
            assemble(g)
        part_copy.wait_recv()
        for g in chunk:
            slots = slice(g * GSLOTS, (g + 1) * GSLOTS)
            both = (amat[slots, :HALF].astype(F32) + prec[slots, :].astype(F32)).astype(BF16)
            tall = jnp.concatenate(
                [both[:, q * QW : (q + 1) * QW] for q in range(QUARTERS)], axis=0
            )
            rsend[g * GROWS : (g + 1) * GROWS, :] = mm(permt[...], tall).astype(BF16)
            for p in range(g * GP, min((g + 1) * GP, PEERS - 1)):
                send_block(rsend, rrecv, p, -1, r_send, r_recv.at[c])
    rrecv[OWN:ALL, :] = rsend[OWN:ALL, :]

    total = jnp.zeros((QUARTERS * SEQ, QW), F32)
    for c, chunk in enumerate(CHUNKS):
        first = chunk[0] * GROWS
        last = (chunk[-1] + 1) * GROWS
        arrived(rrecv.at[pl.ds(first, min(last, OWN) - first)], r_recv.at[c])
        got = rrecv[first:last, :]
        total = total + mm(chi[:, first:last], got) + mm(clo[:, first:last], got)
    for q in range(QUARTERS):
        cols = slice(q * QW, (q + 1) * QW)
        outv[:, cols] = (
            outv[:, cols].astype(F32) + total[q * SEQ : (q + 1) * SEQ, :]
        ).astype(BF16)
    store_out = pltpu.make_async_copy(outv, out_ref, out_sems.at[1])
    store_out.start()
    for copy in started:
        copy.wait_send()
    for sem, buf in ((d_send, sendbuf), (r_send, rsend)):
        sent = buf.at[pl.ds(0, OWN)]
        pltpu.make_async_remote_copy(
            src_ref=sent, dst_ref=sent, send_sem=sem, recv_sem=sem,
            device_id=(ep, other), device_id_type=MESH,
        ).wait_send()
    store_state.wait()
    store_out.wait()


def store(u_in, s_in, u_out, s_out, u_buf, s_buf, in_sems, out_sems):
    pieces = [
        (s_in.at[i, pl.ds(r, 32)], s_buf.at[i, pl.ds(r, 32)], s_out.at[i, pl.ds(r, 32)])
        for i in range(2)
        for r in range(0, SEQ, 32)
    ]
    pieces.append((u_in, u_buf, u_out))
    loads = [pltpu.make_async_copy(a, b, in_sems.at[i]) for i, (a, b, _) in enumerate(pieces)]
    stores = [pltpu.make_async_copy(b, c, out_sems.at[i]) for i, (_, b, c) in enumerate(pieces)]
    for load in loads:
        load.start()
    for load, put in zip(loads, stores):
        load.wait()
        put.start()
    for put in stores:
        put.wait()


def local(
    residual,
    route_ids,
    route_weights,
    carried_state,
    mix_gain,
    in_proj,
    decay_rate,
    frequency,
    step_size,
    input_map,
    output_matrix,
    passthrough_scale,
    out_gain,
    out_proj,
    ffn_gain,
    w_gate,
    w_up,
    w_down,
):
    args = (
        residual,
        route_ids.T,
        route_weights.T,
        decay_rate,
        frequency,
        step_size.reshape(1, -1),
        jnp.swapaxes(input_map, 2, 3).reshape(2, CHAN, -1),
        output_matrix.reshape(2, CHAN, -1),
        mix_gain.reshape(1, -1),
        in_proj,
        carried_state,
        passthrough_scale.reshape(1, -1),
        out_gain.reshape(1, -1),
        out_proj,
        ffn_gain.reshape(2, 1, -1),
        w_gate.reshape(w_gate.shape[1:]),
        w_up.reshape(w_up.shape[1:]),
        w_down.reshape(w_down.shape[1:]),
    )
    dma = pltpu.SemaphoreType.DMA
    vmem = pltpu.VMEM
    out_shape = (
        jax.ShapeDtypeStruct(residual.shape, BF16),
        jax.ShapeDtypeStruct(carried_state.shape, F32),
    )
    results = pl.pallas_call(
        kernel,
        out_shape=out_shape,
        in_specs=[pl.BlockSpec(memory_space=pl.ANY)] * len(args),
        out_specs=(pl.BlockSpec(memory_space=pl.ANY),) * 2,
        scratch_shapes=[
            vmem(residual.shape, BF16),
            vmem(carried_state.shape, F32),
            vmem((2, *residual.shape), BF16),
        ]
        + [vmem(a.shape, a.dtype) for a in args[1:]]
        + [
            vmem((2, CHAN, 512), BF16),
            vmem((2, CHAN, 512), BF16),
            vmem((2, SEQ, CHAN), BF16),
            vmem((2, SEQ, 128), F32),
            vmem((ALL, QUARTERS * SEQ), BF16),
            vmem((QUARTERS * SEQ, ALL), BF16),
            vmem((QUARTERS * SEQ, ALL), BF16),
            vmem((GROWS, GROWS), BF16),
            vmem((GROWS, GROWS), BF16),
            vmem((PAD, QW), BF16),
            vmem((2, PAD, QW), BF16),
            vmem((PAD, QW), BF16),
            vmem((PAD, QW), BF16),
            vmem((PEERS * SLOTS, 2 * HALF), BF16),
            vmem((PEERS * SLOTS, HALF), BF16),
            vmem((PEERS * SLOTS, HALF), BF16),
            vmem((PEERS * SLOTS, HALF), BF16),
            dma((len(args),)),
            dma((2,)),
            dma((3,)),
            dma((3,)),
            dma,
            dma((GROUPS,)),
            dma((GROUPS,)),
            dma((GROUPS,)),
            dma((len(CHUNKS),)),
            dma((len(CHUNKS),)),
            dma,
            dma((len(CHUNKS),)),
        ],
        compiler_params=pltpu.CompilerParams(
            collective_id=0, has_side_effects=True, vmem_limit_bytes=VMEM_LIMIT
        ),
    )(*args)
    return pl.pallas_call(
        store,
        out_shape=out_shape,
        in_specs=[pl.BlockSpec(memory_space=pl.ANY)] * 2,
        out_specs=(pl.BlockSpec(memory_space=pl.ANY),) * 2,
        scratch_shapes=[
            vmem(residual.shape, BF16),
            vmem(carried_state.shape, F32),
            dma((5,)),
            dma((5,)),
        ],
        compiler_params=pltpu.CompilerParams(vmem_limit_bytes=VMEM_LIMIT),
    )(*results)


def solution(mesh):
    placed = (
        P("ep", "tp"),
        P("ep", None),
        P("ep", None),
        P(None, "ep", "tp"),
        P(),
        P(None, "tp"),
        P("tp", None),
        P("tp", None),
        P("tp"),
        P(None, "tp", None, None),
        P(None, "tp", None, None),
        P("tp"),
        P(),
        P(None, "tp"),
        P(),
        P("ep", None, "tp"),
        P("ep", None, "tp"),
        P("ep", "tp", None),
    )
    return jax.shard_map(
        local,
        mesh=mesh,
        in_specs=placed,
        out_specs=(P("ep", "tp"), P(None, "ep", "tp")),
        check_vma=False,
    )
```

time: 57.2 us -> 47.7 us (0.83)
  blocking collectives: 4.77 us -> 0 us
  local copies, waits for them, and re-layouts: 3.86 us -> 0 us
  Pallas kernels: 47.7 us -> 46.9 us
    all_gather x1 -> x0, blocking collectives: 4.77 us -> none  [local(): xg = lax.all_gather(residual, 'tp', axis=0)]
    unnamed x2 -> x0, local copies, waits for them, and re-layouts: 3.86 us -> none
    pallas_call x1 -> x2, Pallas kernels: 47.7 us -> 46.9 us  [the longest x1 44.9 us: local(): pl.pallas_call(kernel, out_shape=out_shape, in_specs=[pl.BlockSpec(memory...]
where the time goes in v2:
time: 47.7 us; the launch traced here: 47.6 us
  Pallas kernels  46.9 us (98%)
  between operations  0.65 us (1%)
    pallas_call x1, Pallas kernels, local(): pl.pallas_call(kernel, out_shape=out_shape, in_specs=[pl.BlockSpec(memory...  44.9 us
    pallas_call x1, Pallas kernels, local(): pl.pallas_call(store, out_shape=out_shape, in_specs=[pl.BlockSpec(memory_...  2.04 us

profile of v2, /device:TPU:1, one launch (start us, length us, event | category | flops | bytes accessed | tf_op | source)
XLA Modules:
  0.0 47.6 jit_solution(8968254897396000911)
XLA Ops:
  0.6 44.9 %shard_map.185 = (bf16[64,1024]{1,0:T(8,128)(2,1)}, f32[2,64,2048]{2,1,0:T(8,128)}) custom-call(bf16[64,1024]{1,0:T(8,128)(2,1)} %x_in.1, s32[4,64]{1,0:T(4,128)} %bitcast.22, f32[4,64]{1,0:T(4,128)} %bitcast.23, f32[32,64]{1,0:T(8,128)} %decay_in.1, f32[32,64]{1,0:T(8,128)} %freq_in.1, f32[1,32]{1,0:T(1,128)} %bitcast.25, f32[2,512,64]{2,1,0:T(8,128)} %bitcast.17, ...), custom_call_target="tpu_custom_call" | custom-call | tf_op jit(solution)/shard_map/pallas_call | solution.py:555
  45.5 2.0 %shard_map.186 = (bf16[64,1024]{1,0:T(8,128)(2,1)}, f32[2,64,2048]{2,1,0:T(8,128)}) custom-call(bf16[64,1024]{1,0:T(8,128)(2,1)} %get-tuple-element.4.u_in, f32[2,64,2048]{2,1,0:T(8,128)} %get-tuple-element.5.s_in), custom_call_target="tpu_custom_call" | custom-call | tf_op jit(solution)/shard_map/pallas_call | solution.py:601

commit v3 on v2

v3 whole, which is shorter than its diff:
```python
import jax
import jax.numpy as jnp
from jax import lax
from jax.experimental import pallas as pl
from jax.experimental.pallas import tpu as pltpu
from jax.sharding import PartitionSpec as P

F32 = jnp.float32
BF16 = jnp.bfloat16
MESH = pl.DeviceIdType.MESH

VMEM_LIMIT = 62 * 1024 * 1024
EPS = 1e-06
LIMIT = 7.0
ALPHA = 1.702

SEQ = 64
HALF = 1024
STATES = 2048
CHAN = 512
PEERS = 64
SLOTS = 6
QUARTERS = 4
QW = HALF // QUARTERS
ROWS = SLOTS * QUARTERS
ALL = PEERS * ROWS
PAD = ALL + 8
OWN = ALL - ROWS
GROUPS = 8
GP = PEERS // GROUPS
GROWS = GP * ROWS
GSLOTS = GP * SLOTS
CHUNKS = ((0, 1), (2, 3, 4), (5, 6, 7))
UNITS = ((0,), (1,), (2, 3, 4), (5, 6, 7))

UNIT_OF = {g: u for u, unit in enumerate(UNITS) for g in unit}


def hops(step):
    return sum(min(d, 4 - d) for d in step)


STEPS = sorted(
    ((dz, dy, dx) for dz in range(4) for dy in range(4) for dx in range(4)), key=hops, reverse=True
)

NT = (((1,), (1,)), ((), ()))


def mm(a, b):
    return jnp.dot(a, b, preferred_element_type=F32)


def mm_nt(a, b):
    return lax.dot_general(a, b, NT, preferred_element_type=F32)


def iota(shape, dim):
    return lax.broadcasted_iota(jnp.int32, shape, dim)


def div_small(v, d):
    return ((v.astype(F32) + 0.5) * (1.0 / d)).astype(jnp.int32)


def kernel(
    x_in,
    ids_in,
    wts_in,
    decay_in,
    freq_in,
    step_in,
    imap_in,
    omap_in,
    mix_gain_in,
    in_proj_in,
    state_in,
    pscale_in,
    out_gain_in,
    out_proj_in,
    ffn_gain_in,
    wg_in,
    wu_in,
    wd_in,
    out_ref,
    nstate_ref,
    outv,
    nstate,
    xv,
    ids,
    wts,
    rates,
    step,
    maps,
    mix_gain,
    in_proj,
    state,
    pscale,
    out_gain,
    out_proj,
    ffn_gain,
    wgu,
    wd,
    inmix,
    outmix,
    actx,
    sqx,
    onehot,
    chi,
    clo,
    perm,
    permt,
    sendbuf,
    recv,
    rsend,
    rrecv,
    amat,
    hid,
    psend,
    prec,
    local_sems,
    hello,
    x_recv,
    d_recv,
    f_recv,
    p_recv,
    r_recv,
):
    ep = lax.axis_index("ep")
    tp = lax.axis_index("tp")
    other = 1 - tp
    z = lax.div(ep, 16)
    y = lax.rem(lax.div(ep, 4), 4)
    x = lax.rem(ep, 4)
    z_at = [lax.rem(z + d, 4) * 16 for d in range(4)]
    y_at = [lax.rem(y + d, 4) * 4 for d in range(4)]
    x_at = [lax.rem(x + d, 4) for d in range(4)]

    def peer_of(p, sign):
        dz, dy, dx = STEPS[p]
        return z_at[sign * dz % 4] + y_at[sign * dy % 4] + x_at[sign * dx % 4]

    pairs = (
        (x_in, xv.at[tp], 0),
        (decay_in, rates.at[0], 1),
        (freq_in, rates.at[1], 1),
        (step_in, step, 2),
        (imap_in, maps.at[0], 3),
        (omap_in, maps.at[1], 3),
        (state_in, state, 4),
        (in_proj_in, in_proj, 5),
        (mix_gain_in, mix_gain, 6),
        (pscale_in, pscale, 7),
        (ids_in, ids, 8),
        (wts_in, wts, 9),
        (out_gain_in, out_gain, 10),
        (out_proj_in, out_proj, 11),
        (ffn_gain_in, ffn_gain, 12),
        (wg_in, wgu.at[0], 0),
        (wu_in, wgu.at[1], 0),
        (wd_in, wd, 1),
    )

    def loaded(ref, sem):
        pltpu.make_async_copy(ref, ref, local_sems.at[sem]).wait()

    loads = [pltpu.make_async_copy(a, b, local_sems.at[i]) for a, b, i in pairs]
    loads[0].start()
    barrier = pltpu.get_barrier_semaphore()

    @pl.when(tp == 0)
    def _():
        pl.semaphore_signal(barrier, inc=1, device_id=(ep, other), device_id_type=MESH)

    for load in loads[1:15]:
        load.start()

    @pl.when(tp == 1)
    def _():
        pl.semaphore_wait(barrier, 1)
        pl.semaphore_signal(hello, inc=1, device_id=(ep, other), device_id_type=MESH)

    @pl.when(tp == 0)
    def _():
        pl.semaphore_wait(hello, 1)

        def greet(i, carry):
            pl.semaphore_signal(
                barrier, inc=1, device_id=(lax.rem(ep + i, PEERS), tp), device_id_type=MESH
            )
            return carry

        lax.fori_loop(1, PEERS, greet, 0)


    loaded(xv.at[tp], 0)

    def to_partner(ref, send, recv_):
        return pltpu.make_async_remote_copy(
            src_ref=ref, dst_ref=ref, send_sem=send, recv_sem=recv_,
            device_id=(ep, other), device_id_type=MESH,
        )

    x_copy = to_partner(xv.at[tp], local_sems.at[0], x_recv.at[2])
    x_copy.start()

    loaded(rates, 1)
    loaded(step, 2)
    rate_real = -rates[0]
    rate_imag = rates[1]
    n_groups, n_state = rate_real.shape
    diag = iota((n_groups, n_groups), 0) == iota((n_groups, n_groups), 1)
    time_step = jnp.sum(jnp.where(diag, step[...], 0.0), axis=1, keepdims=True)
    magnitude = jnp.exp(rate_real * time_step)
    phase = rate_imag * time_step
    bar_real = magnitude * jnp.cos(phase)
    bar_imag = magnitude * jnp.sin(phase)
    denominator = rate_real * rate_real + rate_imag * rate_imag
    shifted = bar_real - 1.0
    coef_real = (shifted * rate_real + bar_imag * rate_imag) / denominator
    coef_imag = (bar_imag * rate_real - shifted * rate_imag) / denominator
    own_group = iota((n_groups, STATES), 0) == (iota((n_groups, STATES), 1) >> 6)

    def as_row(v):
        wide = jnp.concatenate([v] * (STATES // n_state), axis=1)
        return jnp.sum(jnp.where(own_group, wide, 0.0), axis=0, keepdims=True)

    bar_real, bar_imag, coef_real, coef_imag = (
        as_row(v) for v in (bar_real, bar_imag, coef_real, coef_imag)
    )

    same = (iota((128, 512), 0) >> 4) == (iota((128, 512), 1) >> 6)

    def spread_groups(m):
        return jnp.where(same, jnp.concatenate([m] * 8, axis=1), 0.0).astype(BF16)

    loaded(maps, 3)
    for b in range(4):
        rows = slice(b * 128, (b + 1) * 128)
        for i in range(2):
            inmix[i, rows, :] = spread_groups(maps[0, i, rows, :])
        outmix[0, rows, :] = spread_groups(maps[1, 0, rows, :])
        outmix[1, rows, :] = spread_groups(-maps[1, 1, rows, :])

    loaded(state, 4)
    for b in range(4):
        cols = slice(b * 512, (b + 1) * 512)
        hr = state[0, :, cols]
        hi = state[1, :, cols]
        br, bi = bar_real[:, cols], bar_imag[:, cols]
        nstate[0, :, cols] = br * hr - bi * hi
        nstate[1, :, cols] = br * hi + bi * hr
    loaded(in_proj, 5)
    loaded(mix_gain, 6)
    loaded(pscale, 7)
    x_copy.wait()
    x0 = xv[0].astype(F32)
    x1 = xv[1].astype(F32)
    mean_sq = (
        jnp.sum(x0 * x0, axis=1, keepdims=True) + jnp.sum(x1 * x1, axis=1, keepdims=True)
    ) * (1.0 / (2 * HALF))
    scale = lax.rsqrt(mean_sq + EPS)
    n0 = (x0 * scale * mix_gain[:, :HALF]).astype(BF16)
    n1 = (x1 * scale * mix_gain[:, HALF:]).astype(BF16)
    for load in loads[15:]:
        load.start()
    channels = (mm(n0, in_proj[:HALF, :]) + mm(n1, in_proj[HALF:, :])).astype(BF16)
    for b in range(4):
        rows = slice(b * 128, (b + 1) * 128)
        cols = slice(b * 512, (b + 1) * 512)
        ch = channels[:, rows]
        u0 = mm(ch, inmix[0, rows, :])
        u1 = mm(ch, inmix[1, rows, :])
        cr, ci = coef_real[:, cols], coef_imag[:, cols]
        nr = nstate[0, :, cols] + (cr * u0 - ci * u1)
        ni = nstate[1, :, cols] + (cr * u1 + ci * u0)
        nstate[0, :, cols] = nr
        nstate[1, :, cols] = ni
        mixed = (
            mm_nt(nr.astype(BF16), outmix[0, rows, :])
            + mm_nt(ni.astype(BF16), outmix[1, rows, :])
            + pscale[:, rows] * ch.astype(F32)
        )
        actx[tp, :, rows] = jax.nn.gelu(mixed, approximate=True).astype(BF16)

    store_state = pltpu.make_async_copy(nstate, nstate_ref, local_sems.at[5])
    store_state.start()
    act_copy = to_partner(actx.at[tp], local_sems.at[3], x_recv.at[0])
    act_copy.start()

    loaded(ids, 8)
    loaded(wts, 9)
    expert = iota((PEERS, SEQ), 0)
    named = jnp.zeros((PEERS, SEQ), F32)
    weight = jnp.zeros((PEERS, SEQ), F32)
    for k in range(4):
        hit = ids[k : k + 1, :] == expert
        named = named + jnp.where(hit, 1.0, 0.0)
        weight = weight + jnp.where(hit, wts[k : k + 1, :], 0.0)
    earlier = jnp.where(iota((SEQ, SEQ), 0) < iota((SEQ, SEQ), 1), 1.0, 0.0).astype(BF16)
    slot_of = named * (mm(named.astype(BF16), earlier) + 1.0)
    pos = iota((PEERS, PEERS), 0)
    named_at = jnp.zeros((PEERS, PEERS), jnp.int32)
    for p in range(PEERS):
        named_at = jnp.where(pos == p, peer_of(p, 1), named_at)
    order = jnp.where(named_at == iota((PEERS, PEERS), 1), 1.0, 0.0).astype(BF16)
    w_hi = weight.astype(BF16)
    w_lo = (weight - w_hi.astype(F32)).astype(BF16)
    slot_pt = mm(order, slot_of.astype(BF16)).astype(BF16)
    eye = jnp.where(iota((SEQ, SEQ), 0) == iota((SEQ, SEQ), 1), 1.0, 0.0).astype(BF16)

    def turned(v):
        return mm_nt(eye, v).astype(BF16)

    slot_tp = turned(slot_pt)
    whi_tp = turned(mm(order, w_hi).astype(BF16))
    wlo_tp = turned(mm(order, w_lo).astype(BF16))

    slot_p4 = jnp.concatenate([slot_pt] * QUARTERS, axis=1)
    row = iota((GROWS, QUARTERS * SEQ), 0)
    rowp = div_small(row, ROWS)
    rem_row = row - rowp * ROWS
    rowq = div_small(rem_row, SLOTS)
    rows_ = rem_row - rowq * SLOTS
    want = jnp.where(rowq == (iota((GROWS, QUARTERS * SEQ), 1) >> 6), rows_ + 1, -1).astype(F32)
    spread_row = div_small(iota((GROWS, PEERS), 0), ROWS)
    spread_col = iota((GROWS, PEERS), 1)
    for b in range(GROUPS):
        spread = jnp.where(spread_row + b * 8 == spread_col, 1.0, 0.0).astype(BF16)
        onehot[b * GROWS : (b + 1) * GROWS, :] = jnp.where(
            mm(spread, slot_p4) == want, 1.0, 0.0
        ).astype(BF16)

    loaded(out_gain, 10)
    loaded(out_proj, 11)
    loaded(ffn_gain, 12)
    act_copy.wait()
    a0 = actx[0].astype(F32)
    a1 = actx[1].astype(F32)
    mean_sq = (
        jnp.sum(a0 * a0, axis=1, keepdims=True) + jnp.sum(a1 * a1, axis=1, keepdims=True)
    ) * (1.0 / (2 * CHAN))
    scale = lax.rsqrt(mean_sq + EPS)
    s0 = (a0 * scale * out_gain[:, :CHAN]).astype(BF16)
    s1 = (a1 * scale * out_gain[:, CHAN:]).astype(BF16)
    after = (
        xv[tp].astype(F32) + (mm(s0, out_proj[:CHAN, :]) + mm(s1, out_proj[CHAN:, :]))
    ).astype(BF16)
    outv[...] = after
    after32 = after.astype(F32)
    sqx[tp] = jnp.broadcast_to(jnp.sum(after32 * after32, axis=1, keepdims=True), (SEQ, 128))
    sq_copy = to_partner(sqx.at[tp], local_sems.at[4], x_recv.at[1])
    sq_copy.start()

    def block_perm(rdim, cdim):
        r = iota((GROWS, GROWS), rdim)
        c = iota((GROWS, GROWS), cdim)
        rq = div_small(r, GSLOTS)
        rr = r - rq * GSLOTS
        rp = div_small(rr, SLOTS)
        rs = rr - rp * SLOTS
        return jnp.where(rp * ROWS + rq * SLOTS + rs == c, 1.0, 0.0).astype(BF16)

    perm[...] = block_perm(0, 1)
    permt[...] = block_perm(1, 0)

    col = iota((PEERS, ALL), 1)
    spread_t = jnp.where(div_small(col, ROWS) == iota((PEERS, ALL), 0), 1.0, 0.0).astype(BF16)
    c1 = iota((1, ALL), 1)
    c1 = c1 - div_small(c1, ROWS) * ROWS
    cq = div_small(c1, SLOTS)
    cs = (c1 - cq * SLOTS + 1).astype(F32)
    slot_x = mm(slot_tp, spread_t)
    whi_x = mm(whi_tp, spread_t)
    wlo_x = mm(wlo_tp, spread_t)
    hit = slot_x == cs
    for q in range(QUARTERS):
        keep = hit & (cq == q)
        chi[q * SEQ : (q + 1) * SEQ, :] = jnp.where(keep, whi_x, 0.0).astype(BF16)
        clo[q * SEQ : (q + 1) * SEQ, :] = jnp.where(keep, wlo_x, 0.0).astype(BF16)

    sq_copy.wait()
    mean_sq = (sqx[0] + sqx[1])[:, :1] * (1.0 / (2 * HALF))
    expert_in = (after32 * lax.rsqrt(mean_sq + EPS) * ffn_gain[tp]).astype(BF16)
    stacked = jnp.concatenate(
        [expert_in[:, q * QW : (q + 1) * QW] for q in range(QUARTERS)], axis=0
    )

    @pl.when(tp == 0)
    def _():
        pl.semaphore_wait(barrier, PEERS - 1)
        pl.semaphore_signal(hello, inc=1, device_id=(ep, other), device_id_type=MESH)

    @pl.when(tp == 1)
    def _():
        pl.semaphore_wait(hello, 1)

    def send_block(src, dst, p, sign, send, recv_):
        at = pl.ds(p * ROWS, ROWS)
        pltpu.make_async_remote_copy(
            src_ref=src.at[at], dst_ref=dst.at[at], send_sem=send, recv_sem=recv_,
            device_id=(peer_of(p, sign), tp), device_id_type=MESH,
        ).start()

    for b in range(4):
        rows = slice(b * 2 * GROWS, (b + 1) * 2 * GROWS)
        sendbuf[rows, :] = mm(onehot[rows, :], stacked).astype(BF16)
        for p in range(b * 2 * GP, min((b + 1) * 2 * GP, PEERS - 1)):
            send_block(sendbuf, recv.at[tp], p, 1, local_sems.at[7], d_recv.at[UNIT_OF[p // GP]])
    recv[tp, OWN:ALL, :] = sendbuf[OWN:ALL, :]

    loaded(wgu, 0)
    loaded(wd, 1)

    def arrived(ref, sem):
        pltpu.make_async_remote_copy(
            src_ref=ref, dst_ref=ref, send_sem=sem, recv_sem=sem,
            device_id=(ep, other), device_id_type=MESH,
        ).wait_recv()

    forwards = []

    def forward(u):
        first = UNITS[u][0] * GROWS
        last = (UNITS[u][-1] + 1) * GROWS
        arrived(recv.at[tp, pl.ds(first, min(last, OWN) - first)], d_recv.at[u])
        copy = to_partner(recv.at[tp, pl.ds(first, last - first)], local_sems.at[9], f_recv.at[u])
        copy.start()
        forwards.append(copy)

    def assemble(g):
        slots = slice(g * GSLOTS, (g + 1) * GSLOTS)
        for h in range(2):
            moved = mm(perm[...], recv[h, g * GROWS : (g + 1) * GROWS, :]).astype(BF16)
            for q in range(QUARTERS):
                amat[slots, h * HALF + q * QW : h * HALF + (q + 1) * QW] = moved[
                    q * GSLOTS : (q + 1) * GSLOTS, :
                ]

    forward(0)
    forward(1)
    for u in range(2):
        forwards[u].wait_recv()
        assemble(u)
    for c, chunk in enumerate(CHUNKS):
        following = CHUNKS[c + 1] if c + 1 < len(CHUNKS) else ()
        srows = slice(chunk[0] * GSLOTS, (chunk[-1] + 1) * GSLOTS)
        if c == 1:
            forward(3)
        lhs = amat[srows, :]
        for n in range(2):
            at = slice(n * 512, (n + 1) * 512)
            gate = mm(lhs, wgu[0, :, at])
            up = mm(lhs, wgu[1, :, at])
            gated = jnp.minimum(gate, LIMIT)
            act = (jnp.clip(up, -LIMIT, LIMIT) + 1.0) * gated * jax.nn.sigmoid(ALPHA * gated)
            hid[srows, at] = act.astype(BF16)
        if c == 0:
            forward(2)
        lhs = hid[srows, :]
        pieces = 1 if following else 2
        width = HALF // pieces
        parts = []
        for n in range(pieces):
            at = pl.ds(n * width, width)
            wat = pl.ds(pl.multiple_of(other * HALF + n * width, 512), width)
            psend[srows, at] = mm(lhs, wd[:, wat]).astype(BF16)
            part_copy = pltpu.make_async_remote_copy(
                src_ref=psend.at[srows, at], dst_ref=prec.at[srows, at],
                send_sem=local_sems.at[10], recv_sem=p_recv.at[c + n],
                device_id=(ep, other), device_id_type=MESH,
            )
            part_copy.start()
            parts.append(part_copy)
        if c == 1:
            forwards[3].wait_recv()
        wat = pl.ds(pl.multiple_of(tp * HALF, HALF), HALF)
        amat[srows, :HALF] = mm(lhs, wd[:, wat]).astype(BF16)
        if c == 0:
            forwards[2].wait_recv()
        for g in following:
            assemble(g)
        for part_copy in parts:
            part_copy.wait_recv()
        for g in chunk:
            slots = slice(g * GSLOTS, (g + 1) * GSLOTS)
            both = (amat[slots, :HALF].astype(F32) + prec[slots, :].astype(F32)).astype(BF16)
            tall = jnp.concatenate(
                [both[:, q * QW : (q + 1) * QW] for q in range(QUARTERS)], axis=0
            )
            rsend[g * GROWS : (g + 1) * GROWS, :] = mm(permt[...], tall).astype(BF16)
        for g in chunk:
            for p in range(g * GP, min((g + 1) * GP, PEERS - 1)):
                send_block(rsend, rrecv, p, -1, local_sems.at[8], r_recv.at[c])
    rrecv[OWN:ALL, :] = rsend[OWN:ALL, :]

    total = jnp.zeros((QUARTERS * SEQ, QW), F32)
    for c, chunk in enumerate(CHUNKS):
        first = chunk[0] * GROWS
        last = (chunk[-1] + 1) * GROWS
        arrived(rrecv.at[pl.ds(first, min(last, OWN) - first)], r_recv.at[c])
        got = rrecv[first:last, :]
        total = total + mm(chi[:, first:last], got) + mm(clo[:, first:last], got)
    for q in range(QUARTERS):
        cols = slice(q * QW, (q + 1) * QW)
        outv[:, cols] = (
            outv[:, cols].astype(F32) + total[q * SEQ : (q + 1) * SEQ, :]
        ).astype(BF16)
    store_out = pltpu.make_async_copy(outv, out_ref, local_sems.at[6])
    store_out.start()
    for sem, sent in (
        (7, sendbuf.at[pl.ds(0, OWN)]),
        (8, rsend.at[pl.ds(0, OWN)]),
        (9, recv.at[tp, pl.ds(0, ALL)]),
        (10, psend),
    ):
        pltpu.make_async_remote_copy(
            src_ref=sent, dst_ref=sent, send_sem=local_sems.at[sem], recv_sem=local_sems.at[sem],
            device_id=(ep, other), device_id_type=MESH,
        ).wait_send()
    store_state.wait()
    store_out.wait()


def store(u_in, s_in, u_out, s_out, u_buf, s_buf, in_sems, out_sems):
    pieces = [
        (s_in.at[i, pl.ds(r, 32)], s_buf.at[i, pl.ds(r, 32)], s_out.at[i, pl.ds(r, 32)])
        for i in range(2)
        for r in range(0, SEQ, 32)
    ]
    pieces.append((u_in, u_buf, u_out))
    loads = [pltpu.make_async_copy(a, b, in_sems.at[i]) for i, (a, b, _) in enumerate(pieces)]
    stores = [pltpu.make_async_copy(b, c, out_sems.at[i]) for i, (_, b, c) in enumerate(pieces)]
    for load in loads:
        load.start()
    for load, put in zip(loads, stores):
        load.wait()
        put.start()
    for put in stores:
        put.wait()


def local(
    residual,
    route_ids,
    route_weights,
    carried_state,
    mix_gain,
    in_proj,
    decay_rate,
    frequency,
    step_size,
    input_map,
    output_matrix,
    passthrough_scale,
    out_gain,
    out_proj,
    ffn_gain,
    w_gate,
    w_up,
    w_down,
):
    ids, wts = route_ids.T, route_weights.T
    maps = (
        jnp.swapaxes(input_map, 2, 3).reshape(2, CHAN, -1),
        output_matrix.reshape(2, CHAN, -1),
    )
    args = (
        residual,
        ids,
        wts,
        decay_rate,
        frequency,
        step_size.reshape(1, -1),
        *maps,
        mix_gain.reshape(1, -1),
        in_proj,
        carried_state,
        passthrough_scale.reshape(1, -1),
        out_gain.reshape(1, -1),
        out_proj,
        ffn_gain.reshape(2, 1, -1),
        w_gate.reshape(w_gate.shape[1:]),
        w_up.reshape(w_up.shape[1:]),
        w_down.reshape(w_down.shape[1:]),
    )
    dma = pltpu.SemaphoreType.DMA
    vmem = pltpu.VMEM
    out_shape = (
        jax.ShapeDtypeStruct(residual.shape, BF16),
        jax.ShapeDtypeStruct(carried_state.shape, F32),
    )
    results = pl.pallas_call(
        kernel,
        out_shape=out_shape,
        in_specs=[pl.BlockSpec(memory_space=pl.ANY)] * len(args),
        out_specs=(pl.BlockSpec(memory_space=pl.ANY),) * 2,
        scratch_shapes=[
            vmem(residual.shape, BF16),
            vmem(carried_state.shape, F32),
            vmem((2, *residual.shape), BF16),
        ]
        + [vmem(a.shape, a.dtype) for a in (ids, wts)]
        + [
            vmem((2, *decay_rate.shape), F32),
            vmem((1, step_size.shape[0]), F32),
            vmem((2, *maps[0].shape), F32),
            vmem((1, mix_gain.shape[0]), F32),
            vmem(in_proj.shape, BF16),
            vmem(carried_state.shape, F32),
            vmem((1, CHAN), F32),
            vmem((1, 2 * CHAN), F32),
            vmem(out_proj.shape, BF16),
            vmem((2, 1, HALF), F32),
            vmem((2, *w_gate.shape[1:]), BF16),
            vmem(w_down.shape[1:], BF16),
            vmem((2, CHAN, 512), BF16),
            vmem((2, CHAN, 512), BF16),
            vmem((2, SEQ, CHAN), BF16),
            vmem((2, SEQ, 128), F32),
            vmem((ALL, QUARTERS * SEQ), BF16),
            vmem((QUARTERS * SEQ, ALL), BF16),
            vmem((QUARTERS * SEQ, ALL), BF16),
            vmem((GROWS, GROWS), BF16),
            vmem((GROWS, GROWS), BF16),
            vmem((PAD, QW), BF16),
            vmem((2, PAD, QW), BF16),
            vmem((PAD, QW), BF16),
            vmem((PAD, QW), BF16),
            vmem((PEERS * SLOTS, 2 * HALF), BF16),
            vmem((PEERS * SLOTS, HALF), BF16),
            vmem((PEERS * SLOTS, HALF), BF16),
            vmem((PEERS * SLOTS, HALF), BF16),
            dma((13,)),
            pltpu.SemaphoreType.REGULAR,
            dma((3,)),
            dma((len(UNITS),)),
            dma((len(UNITS),)),
            dma((len(CHUNKS) + 1,)),
            dma((len(CHUNKS),)),
        ],
        compiler_params=pltpu.CompilerParams(
            collective_id=0, has_side_effects=True, vmem_limit_bytes=VMEM_LIMIT
        ),
    )(*args)
    return pl.pallas_call(
        store,
        out_shape=out_shape,
        in_specs=[pl.BlockSpec(memory_space=pl.ANY)] * 2,
        out_specs=(pl.BlockSpec(memory_space=pl.ANY),) * 2,
        scratch_shapes=[
            vmem(residual.shape, BF16),
            vmem(carried_state.shape, F32),
            dma((5,)),
            dma((5,)),
        ],
        compiler_params=pltpu.CompilerParams(vmem_limit_bytes=VMEM_LIMIT),
    )(*results)


def solution(mesh):
    placed = (
        P("ep", "tp"),
        P("ep", None),
        P("ep", None),
        P(None, "ep", "tp"),
        P(),
        P(None, "tp"),
        P("tp", None),
        P("tp", None),
        P("tp"),
        P(None, "tp", None, None),
        P(None, "tp", None, None),
        P("tp"),
        P(),
        P(None, "tp"),
        P(),
        P("ep", None, "tp"),
        P("ep", None, "tp"),
        P("ep", "tp", None),
    )
    return jax.shard_map(
        local,
        mesh=mesh,
        in_specs=placed,
        out_specs=(P("ep", "tp"), P(None, "ep", "tp")),
        check_vma=False,
    )
```

time: 47.7 us -> 43.4 us (0.910)
  Pallas kernels: 46.9 us -> 42.6 us
    pallas_call x1, Pallas kernels: 44.9 us -> 40.6 us  [local(): pl.pallas_call(kernel, out_shape=out_shape, in_specs=[pl.BlockSpec(memory...]
where the time goes in v3:
time: 43.4 us; the launch traced here: 43.3 us
  Pallas kernels  42.6 us (98%)
  between operations  0.65 us (1%)
    pallas_call x1, Pallas kernels, local(): pl.pallas_call(kernel, out_shape=out_shape, in_specs=[pl.BlockSpec(memory...  40.6 us
    pallas_call x1, Pallas kernels, local(): pl.pallas_call(store, out_shape=out_shape, in_specs=[pl.BlockSpec(memory_...  2.04 us

profile of v3, /device:TPU:1, one launch (start us, length us, event | category | flops | bytes accessed | tf_op | source)
XLA Modules:
  0.0 43.3 jit_solution(15701527144453215397)
XLA Ops:
  0.6 40.6 %shard_map.185 = (bf16[64,1024]{1,0:T(8,128)(2,1)}, f32[2,64,2048]{2,1,0:T(8,128)}) custom-call(bf16[64,1024]{1,0:T(8,128)(2,1)} %x_in.1, s32[4,64]{1,0:T(4,128)} %bitcast.22, f32[4,64]{1,0:T(4,128)} %bitcast.23, f32[32,64]{1,0:T(8,128)} %decay_in.1, f32[32,64]{1,0:T(8,128)} %freq_in.1, f32[1,32]{1,0:T(1,128)} %bitcast.25, f32[2,512,64]{2,1,0:T(8,128)} %bitcast.17, ...), custom_call_target="tpu_custom_call" | custom-call | tf_op jit(solution)/shard_map/pallas_call | solution.py:593
  41.2 2.0 %shard_map.186 = (bf16[64,1024]{1,0:T(8,128)(2,1)}, f32[2,64,2048]{2,1,0:T(8,128)}) custom-call(bf16[64,1024]{1,0:T(8,128)(2,1)} %get-tuple-element.4.u_in, f32[2,64,2048]{2,1,0:T(8,128)} %get-tuple-element.5.s_in), custom_call_target="tpu_custom_call" | custom-call | tf_op jit(solution)/shard_map/pallas_call | solution.py:646

commit v4 on v3

--- a/solution.py
+++ b/solution.py
@@ -9,6 +9,7 @@
 BF16 = jnp.bfloat16
 MESH = pl.DeviceIdType.MESH
 
+AHEAD = 2
 VMEM_LIMIT = 62 * 1024 * 1024
 EPS = 1e-06
 LIMIT = 7.0
@@ -107,7 +108,6 @@
     sqx,
     onehot,
     chi,
-    clo,
     perm,
     permt,
     sendbuf,
@@ -116,6 +116,7 @@
     rrecv,
     amat,
     hid,
+    own,
     psend,
     prec,
     local_sems,
@@ -142,20 +143,20 @@
 
     pairs = (
         (x_in, xv.at[tp], 0),
+        (in_proj_in, in_proj, 5),
         (decay_in, rates.at[0], 1),
         (freq_in, rates.at[1], 1),
         (step_in, step, 2),
         (imap_in, maps.at[0], 3),
         (omap_in, maps.at[1], 3),
+        (mix_gain_in, mix_gain, 6),
         (state_in, state, 4),
-        (in_proj_in, in_proj, 5),
-        (mix_gain_in, mix_gain, 6),
         (pscale_in, pscale, 7),
         (ids_in, ids, 8),
         (wts_in, wts, 9),
         (out_gain_in, out_gain, 10),
+        (ffn_gain_in, ffn_gain, 12),
         (out_proj_in, out_proj, 11),
-        (ffn_gain_in, ffn_gain, 12),
         (wg_in, wgu.at[0], 0),
         (wu_in, wgu.at[1], 0),
         (wd_in, wd, 1),
@@ -172,7 +173,7 @@
     def _():
         pl.semaphore_signal(barrier, inc=1, device_id=(ep, other), device_id_type=MESH)
 
-    for load in loads[1:15]:
+    for load in loads[1:14]:
         load.start()
 
     @pl.when(tp == 1)
@@ -262,26 +263,30 @@
     scale = lax.rsqrt(mean_sq + EPS)
     n0 = (x0 * scale * mix_gain[:, :HALF]).astype(BF16)
     n1 = (x1 * scale * mix_gain[:, HALF:]).astype(BF16)
-    for load in loads[15:]:
+    for load in loads[14:]:
         load.start()
     channels = (mm(n0, in_proj[:HALF, :]) + mm(n1, in_proj[HALF:, :])).astype(BF16)
-    for b in range(4):
-        rows = slice(b * 128, (b + 1) * 128)
-        cols = slice(b * 512, (b + 1) * 512)
-        ch = channels[:, rows]
-        u0 = mm(ch, inmix[0, rows, :])
-        u1 = mm(ch, inmix[1, rows, :])
+    spans = [(slice(b * 128, (b + 1) * 128), slice(b * 512, (b + 1) * 512)) for b in range(4)]
+    pushes = [
+        (mm(channels[:, rows], inmix[0, rows, :]), mm(channels[:, rows], inmix[1, rows, :]))
+        for rows, _ in spans
+    ]
+    states = []
+    for (rows, cols), (u0, u1) in zip(spans, pushes):
         cr, ci = coef_real[:, cols], coef_imag[:, cols]
         nr = nstate[0, :, cols] + (cr * u0 - ci * u1)
         ni = nstate[1, :, cols] + (cr * u1 + ci * u0)
         nstate[0, :, cols] = nr
         nstate[1, :, cols] = ni
-        mixed = (
-            mm_nt(nr.astype(BF16), outmix[0, rows, :])
-            + mm_nt(ni.astype(BF16), outmix[1, rows, :])
-            + pscale[:, rows] * ch.astype(F32)
-        )
-        actx[tp, :, rows] = jax.nn.gelu(mixed, approximate=True).astype(BF16)
+        states.append((nr.astype(BF16), ni.astype(BF16)))
+    mixed = jnp.concatenate(
+        [
+            mm_nt(nr, outmix[0, rows, :]) + mm_nt(ni, outmix[1, rows, :])
+            for (rows, _), (nr, ni) in zip(spans, states)
+        ],
+        axis=1,
+    ) + pscale[...] * channels.astype(F32)
+    actx[tp] = jax.nn.gelu(mixed, approximate=True).astype(BF16)
 
     store_state = pltpu.make_async_copy(nstate, nstate_ref, local_sems.at[5])
     store_state.start()
@@ -305,7 +310,6 @@
         named_at = jnp.where(pos == p, peer_of(p, 1), named_at)
     order = jnp.where(named_at == iota((PEERS, PEERS), 1), 1.0, 0.0).astype(BF16)
     w_hi = weight.astype(BF16)
-    w_lo = (weight - w_hi.astype(F32)).astype(BF16)
     slot_pt = mm(order, slot_of.astype(BF16)).astype(BF16)
     eye = jnp.where(iota((SEQ, SEQ), 0) == iota((SEQ, SEQ), 1), 1.0, 0.0).astype(BF16)
 
@@ -314,7 +318,6 @@
 
     slot_tp = turned(slot_pt)
     whi_tp = turned(mm(order, w_hi).astype(BF16))
-    wlo_tp = turned(mm(order, w_lo).astype(BF16))
 
     slot_p4 = jnp.concatenate([slot_pt] * QUARTERS, axis=1)
     row = iota((GROWS, QUARTERS * SEQ), 0)
@@ -352,6 +355,38 @@
     sq_copy = to_partner(sqx.at[tp], local_sems.at[4], x_recv.at[1])
     sq_copy.start()
 
+    @pl.when(tp == 0)
+    def _():
+        pl.semaphore_wait(barrier, PEERS - 1)
+        pl.semaphore_signal(hello, inc=1, device_id=(ep, other), device_id_type=MESH)
+
+    def send_block(src, dst, p, sign, send, recv_):
+        at = pl.ds(p * ROWS, ROWS)
+        pltpu.make_async_remote_copy(
+            src_ref=src.at[at], dst_ref=dst.at[at], send_sem=send, recv_sem=recv_,
+            device_id=(peer_of(p, sign), tp), device_id_type=MESH,
+        ).start()
+
+    def gather(b, values):
+        stacked = jnp.concatenate(
+            [values[:, q * QW : (q + 1) * QW] for q in range(QUARTERS)], axis=0
+        )
+        rows = slice(b[0] * GROWS, (b[-1] + 1) * GROWS)
+        sendbuf[rows, :] = mm(onehot[rows, :], stacked).astype(BF16)
+
+    def dispatch(b):
+        for p in range(b[0] * GP, min((b[-1] + 1) * GP, PEERS - 1)):
+            send_block(sendbuf, recv.at[tp], p, 1, local_sems.at[7], d_recv.at[UNIT_OF[p // GP]])
+
+
+    gather(CHUNKS[0], after)
+
+    @pl.when(tp == 1)
+    def _():
+        pl.semaphore_wait(hello, 1)
+
+    dispatch(CHUNKS[0])
+
     def block_perm(rdim, cdim):
         r = iota((GROWS, GROWS), rdim)
         c = iota((GROWS, GROWS), cdim)
@@ -364,6 +399,14 @@
     perm[...] = block_perm(0, 1)
     permt[...] = block_perm(1, 0)
 
+    sq_copy.wait()
+    mean_sq = (sqx[0] + sqx[1])[:, :1] * (1.0 / (2 * HALF))
+    expert_in = (after32 * lax.rsqrt(mean_sq + EPS) * ffn_gain[tp]).astype(BF16)
+    for b in CHUNKS[1:]:
+        gather(b, expert_in)
+        dispatch(b)
+    recv[tp, OWN:ALL, :] = sendbuf[OWN:ALL, :]
+
     col = iota((PEERS, ALL), 1)
     spread_t = jnp.where(div_small(col, ROWS) == iota((PEERS, ALL), 0), 1.0, 0.0).astype(BF16)
     c1 = iota((1, ALL), 1)
@@ -372,42 +415,10 @@
     cs = (c1 - cq * SLOTS + 1).astype(F32)
     slot_x = mm(slot_tp, spread_t)
     whi_x = mm(whi_tp, spread_t)
-    wlo_x = mm(wlo_tp, spread_t)
     hit = slot_x == cs
     for q in range(QUARTERS):
         keep = hit & (cq == q)
         chi[q * SEQ : (q + 1) * SEQ, :] = jnp.where(keep, whi_x, 0.0).astype(BF16)
-        clo[q * SEQ : (q + 1) * SEQ, :] = jnp.where(keep, wlo_x, 0.0).astype(BF16)
-
-    sq_copy.wait()
-    mean_sq = (sqx[0] + sqx[1])[:, :1] * (1.0 / (2 * HALF))
-    expert_in = (after32 * lax.rsqrt(mean_sq + EPS) * ffn_gain[tp]).astype(BF16)
-    stacked = jnp.concatenate(
-        [expert_in[:, q * QW : (q + 1) * QW] for q in range(QUARTERS)], axis=0
-    )
-
-    @pl.when(tp == 0)
-    def _():
-        pl.semaphore_wait(barrier, PEERS - 1)
-        pl.semaphore_signal(hello, inc=1, device_id=(ep, other), device_id_type=MESH)
-
-    @pl.when(tp == 1)
-    def _():
-        pl.semaphore_wait(hello, 1)
-
-    def send_block(src, dst, p, sign, send, recv_):
-        at = pl.ds(p * ROWS, ROWS)
-        pltpu.make_async_remote_copy(
-            src_ref=src.at[at], dst_ref=dst.at[at], send_sem=send, recv_sem=recv_,
-            device_id=(peer_of(p, sign), tp), device_id_type=MESH,
-        ).start()
-
-    for b in range(4):
-        rows = slice(b * 2 * GROWS, (b + 1) * 2 * GROWS)
-        sendbuf[rows, :] = mm(onehot[rows, :], stacked).astype(BF16)
-        for p in range(b * 2 * GP, min((b + 1) * 2 * GP, PEERS - 1)):
-            send_block(sendbuf, recv.at[tp], p, 1, local_sems.at[7], d_recv.at[UNIT_OF[p // GP]])
-    recv[tp, OWN:ALL, :] = sendbuf[OWN:ALL, :]
 
     loaded(wgu, 0)
     loaded(wd, 1)
@@ -418,80 +429,108 @@
             device_id=(ep, other), device_id_type=MESH,
         ).wait_recv()
 
-    forwards = []
-
-    def forward(u):
+    def passed_on(u):
         first = UNITS[u][0] * GROWS
         last = (UNITS[u][-1] + 1) * GROWS
+        return first, last, to_partner(
+            recv.at[tp, pl.ds(first, last - first)], local_sems.at[9], f_recv.at[u]
+        )
+
+    def forward(u):
+        first, last, copy = passed_on(u)
         arrived(recv.at[tp, pl.ds(first, min(last, OWN) - first)], d_recv.at[u])
-        copy = to_partner(recv.at[tp, pl.ds(first, last - first)], local_sems.at[9], f_recv.at[u])
         copy.start()
-        forwards.append(copy)
 
     def assemble(g):
         slots = slice(g * GSLOTS, (g + 1) * GSLOTS)
-        for h in range(2):
-            moved = mm(perm[...], recv[h, g * GROWS : (g + 1) * GROWS, :]).astype(BF16)
-            for q in range(QUARTERS):
-                amat[slots, h * HALF + q * QW : h * HALF + (q + 1) * QW] = moved[
-                    q * GSLOTS : (q + 1) * GSLOTS, :
-                ]
-
-    forward(0)
-    forward(1)
-    for u in range(2):
-        forwards[u].wait_recv()
-        assemble(u)
-    for c, chunk in enumerate(CHUNKS):
-        following = CHUNKS[c + 1] if c + 1 < len(CHUNKS) else ()
-        srows = slice(chunk[0] * GSLOTS, (chunk[-1] + 1) * GSLOTS)
-        if c == 1:
-            forward(3)
-        lhs = amat[srows, :]
-        for n in range(2):
-            at = slice(n * 512, (n + 1) * 512)
-            gate = mm(lhs, wgu[0, :, at])
-            up = mm(lhs, wgu[1, :, at])
-            gated = jnp.minimum(gate, LIMIT)
-            act = (jnp.clip(up, -LIMIT, LIMIT) + 1.0) * gated * jax.nn.sigmoid(ALPHA * gated)
-            hid[srows, at] = act.astype(BF16)
-        if c == 0:
-            forward(2)
-        lhs = hid[srows, :]
-        pieces = 1 if following else 2
-        width = HALF // pieces
-        parts = []
-        for n in range(pieces):
-            at = pl.ds(n * width, width)
-            wat = pl.ds(pl.multiple_of(other * HALF + n * width, 512), width)
-            psend[srows, at] = mm(lhs, wd[:, wat]).astype(BF16)
-            part_copy = pltpu.make_async_remote_copy(
-                src_ref=psend.at[srows, at], dst_ref=prec.at[srows, at],
-                send_sem=local_sems.at[10], recv_sem=p_recv.at[c + n],
-                device_id=(ep, other), device_id_type=MESH,
-            )
-            part_copy.start()
-            parts.append(part_copy)
-        if c == 1:
-            forwards[3].wait_recv()
-        wat = pl.ds(pl.multiple_of(tp * HALF, HALF), HALF)
-        amat[srows, :HALF] = mm(lhs, wd[:, wat]).astype(BF16)
-        if c == 0:
-            forwards[2].wait_recv()
-        for g in following:
-            assemble(g)
-        for part_copy in parts:
-            part_copy.wait_recv()
-        for g in chunk:
-            slots = slice(g * GSLOTS, (g + 1) * GSLOTS)
-            both = (amat[slots, :HALF].astype(F32) + prec[slots, :].astype(F32)).astype(BF16)
-            tall = jnp.concatenate(
-                [both[:, q * QW : (q + 1) * QW] for q in range(QUARTERS)], axis=0
-            )
-            rsend[g * GROWS : (g + 1) * GROWS, :] = mm(permt[...], tall).astype(BF16)
-        for g in chunk:
-            for p in range(g * GP, min((g + 1) * GP, PEERS - 1)):
-                send_block(rsend, rrecv, p, -1, local_sems.at[8], r_recv.at[c])
+        moved = [mm(perm[...], recv[h, g * GROWS : (g + 1) * GROWS, :]) for h in range(2)]
+        pieces = [
+            (h, slice(q * QW, (q + 1) * QW), moved[h][q * GSLOTS : (q + 1) * GSLOTS, :])
+            for h in range(2)
+            for q in range(QUARTERS)
+        ]
+        if g in CHUNKS[0]:
+            squares = pieces[0][2] * pieces[0][2]
+            for _, _, piece in pieces[1:]:
+                squares = squares + piece * piece
+            mean_sq = jnp.sum(squares, axis=1, keepdims=True) * (1.0 / (2 * HALF))
+            scale = lax.rsqrt(mean_sq + EPS)
+            pieces = [(h, at, piece * scale * ffn_gain[h, :, at]) for h, at, piece in pieces]
+        for h, at, piece in pieces:
+            amat[slots, h * HALF + at.start : h * HALF + at.stop] = piece.astype(BF16)
+
+    def experts(order):
+        units_of = [[u for u in range(len(UNITS)) if UNITS[u][0] in CHUNKS[c]] for c in order] + [[]]
+        for u in units_of[0]:
+            forward(u)
+        for u in units_of[0]:
+            passed_on(u)[2].wait_recv()
+            for g in UNITS[u]:
+                assemble(g)
+
+        def units(c, halves):
+            srows = slice(CHUNKS[c][0] * GSLOTS, (CHUNKS[c][-1] + 1) * GSLOTS)
+            lhs = amat[srows, :]
+            for n in halves:
+                at = slice(n * 512, (n + 1) * 512)
+                gate = mm(lhs, wgu[0, :, at])
+                up = mm(lhs, wgu[1, :, at])
+                gated = jnp.minimum(gate, LIMIT)
+                act = (jnp.clip(up, -LIMIT, LIMIT) + 1.0) * gated * jax.nn.sigmoid(ALPHA * gated)
+                hid[srows, at] = act.astype(BF16)
+
+        for i, c in enumerate(order):
+            chunk = CHUNKS[c]
+            last = i + 1 == len(order)
+            srows = slice(chunk[0] * GSLOTS, (chunk[-1] + 1) * GSLOTS)
+            if i == 1:
+                for u in units_of[i + 1]:
+                    forward(u)
+            units(c, (1,) if i >= AHEAD else (0, 1))
+            if i == 0:
+                for u in units_of[i + 1]:
+                    forward(u)
+            lhs = hid[srows, :]
+            pieces = 2 if last else 1
+            width = HALF // pieces
+            parts = []
+            for n in range(pieces):
+                at = pl.ds(n * width, width)
+                wat = pl.ds(pl.multiple_of(other * HALF + n * width, 512), width)
+                psend[srows, at] = mm(lhs, wd[:, wat]).astype(BF16)
+                part_copy = pltpu.make_async_remote_copy(
+                    src_ref=psend.at[srows, at], dst_ref=prec.at[srows, at],
+                    send_sem=local_sems.at[10], recv_sem=p_recv.at[i + n],
+                    device_id=(ep, other), device_id_type=MESH,
+                )
+                part_copy.start()
+                parts.append(part_copy)
+            if i == 1:
+                for u in units_of[i + 1]:
+                    passed_on(u)[2].wait_recv()
+            own[srows, :] = mm(lhs, wd[:, pl.ds(pl.multiple_of(tp * HALF, HALF), HALF)]).astype(BF16)
+            if i == 0:
+                for u in units_of[i + 1]:
+                    passed_on(u)[2].wait_recv()
+            for u in units_of[i + 1]:
+                for g in UNITS[u]:
+                    assemble(g)
+            if not last and i + 1 >= AHEAD:
+                units(order[i + 1], (0,))
+            for part_copy in parts:
+                part_copy.wait_recv()
+            for g in chunk:
+                slots = slice(g * GSLOTS, (g + 1) * GSLOTS)
+                both = (own[slots, :].astype(F32) + prec[slots, :].astype(F32)).astype(BF16)
+                tall = jnp.concatenate(
+                    [both[:, q * QW : (q + 1) * QW] for q in range(QUARTERS)], axis=0
+                )
+                rsend[g * GROWS : (g + 1) * GROWS, :] = mm(permt[...], tall).astype(BF16)
+            for g in chunk:
+                for p in range(g * GP, min((g + 1) * GP, PEERS - 1)):
+                    send_block(rsend, rrecv, p, -1, local_sems.at[8], r_recv.at[c])
+
+    experts(tuple(range(len(CHUNKS))))
     rrecv[OWN:ALL, :] = rsend[OWN:ALL, :]
 
     total = jnp.zeros((QUARTERS * SEQ, QW), F32)
@@ -500,7 +539,7 @@
         last = (chunk[-1] + 1) * GROWS
         arrived(rrecv.at[pl.ds(first, min(last, OWN) - first)], r_recv.at[c])
         got = rrecv[first:last, :]
-        total = total + mm(chi[:, first:last], got) + mm(clo[:, first:last], got)
+        total = total + mm(chi[:, first:last], got)
     for q in range(QUARTERS):
         cols = slice(q * QW, (q + 1) * QW)
         outv[:, cols] = (
@@ -620,7 +659,6 @@
             vmem((2, SEQ, 128), F32),
             vmem((ALL, QUARTERS * SEQ), BF16),
             vmem((QUARTERS * SEQ, ALL), BF16),
-            vmem((QUARTERS * SEQ, ALL), BF16),
             vmem((GROWS, GROWS), BF16),
             vmem((GROWS, GROWS), BF16),
             vmem((PAD, QW), BF16),
@@ -628,6 +666,7 @@
             vmem((PAD, QW), BF16),
             vmem((PAD, QW), BF16),
             vmem((PEERS * SLOTS, 2 * HALF), BF16),
+            vmem((PEERS * SLOTS, HALF), BF16),
             vmem((PEERS * SLOTS, HALF), BF16),
             vmem((PEERS * SLOTS, HALF), BF16),
             vmem((PEERS * SLOTS, HALF), BF16),

time: 43.4 us -> 42.2 us (0.972)
  Pallas kernels: 42.6 us -> 41.4 us
    pallas_call x1, Pallas kernels: 40.6 us -> 39.4 us  [local(): pl.pallas_call(kernel, out_shape=out_shape, in_specs=[pl.BlockSpec(memory...]
where the time goes in v4:
time: 42.2 us; the launch traced here: 42.1 us
  Pallas kernels  41.4 us (98%)
  between operations  0.65 us (2%)
    pallas_call x1, Pallas kernels, local(): pl.pallas_call(kernel, out_shape=out_shape, in_specs=[pl.BlockSpec(memory...  39.4 us
    pallas_call x1, Pallas kernels, local(): pl.pallas_call(store, out_shape=out_shape, in_specs=[pl.BlockSpec(memory_...  2.04 us

profile of v4, /device:TPU:1, one launch (start us, length us, event | category | flops | bytes accessed | tf_op | source)
XLA Modules:
  0.0 42.1 jit_solution(764657116497906407)
XLA Ops:
  0.6 39.4 %shard_map.185 = (bf16[64,1024]{1,0:T(8,128)(2,1)}, f32[2,64,2048]{2,1,0:T(8,128)}) custom-call(bf16[64,1024]{1,0:T(8,128)(2,1)} %x_in.1, s32[4,64]{1,0:T(4,128)} %bitcast.22, f32[4,64]{1,0:T(4,128)} %bitcast.23, f32[32,64]{1,0:T(8,128)} %decay_in.1, f32[32,64]{1,0:T(8,128)} %freq_in.1, f32[1,32]{1,0:T(1,128)} %bitcast.25, f32[2,512,64]{2,1,0:T(8,128)} %bitcast.17, ...), custom_call_target="tpu_custom_call" | custom-call | tf_op jit(solution)/shard_map/pallas_call | solution.py:632
  40.0 2.0 %shard_map.186 = (bf16[64,1024]{1,0:T(8,128)(2,1)}, f32[2,64,2048]{2,1,0:T(8,128)}) custom-call(bf16[64,1024]{1,0:T(8,128)(2,1)} %get-tuple-element.4.u_in, f32[2,64,2048]{2,1,0:T(8,128)} %get-tuple-element.5.s_in), custom_call_target="tpu_custom_call" | custom-call | tf_op jit(solution)/shard_map/pallas_call | solution.py:685

commit v5 on v4

--- a/solution.py
+++ b/solution.py
@@ -509,12 +509,10 @@
                 for u in units_of[i + 1]:
                     passed_on(u)[2].wait_recv()
             own[srows, :] = mm(lhs, wd[:, pl.ds(pl.multiple_of(tp * HALF, HALF), HALF)]).astype(BF16)
-            if i == 0:
+            if i > 0:
                 for u in units_of[i + 1]:
-                    passed_on(u)[2].wait_recv()
-            for u in units_of[i + 1]:
-                for g in UNITS[u]:
-                    assemble(g)
+                    for g in UNITS[u]:
+                        assemble(g)
             if not last and i + 1 >= AHEAD:
                 units(order[i + 1], (0,))
             for part_copy in parts:
@@ -529,6 +527,12 @@
             for g in chunk:
                 for p in range(g * GP, min((g + 1) * GP, PEERS - 1)):
                     send_block(rsend, rrecv, p, -1, local_sems.at[8], r_recv.at[c])
+            if i == 0:
+                for u in units_of[1]:
+                    passed_on(u)[2].wait_recv()
+                for u in units_of[1]:
+                    for g in UNITS[u]:
+                        assemble(g)
 
     experts(tuple(range(len(CHUNKS))))
     rrecv[OWN:ALL, :] = rsend[OWN:ALL, :]

time: 42.2 us -> 42.1 us (level)
  no operation moved by 1% of the time
where the time goes in v5:
time: 42.1 us; the launch traced here: 41.9 us
  Pallas kernels  41.3 us (98%)
  between operations  0.65 us (2%)
    pallas_call x1, Pallas kernels, local(): pl.pallas_call(kernel, out_shape=out_shape, in_specs=[pl.BlockSpec(memory...  39.3 us
    pallas_call x1, Pallas kernels, local(): pl.pallas_call(store, out_shape=out_shape, in_specs=[pl.BlockSpec(memory_...  2.04 us

profile of v5, /device:TPU:1, one launch (start us, length us, event | category | flops | bytes accessed | tf_op | source)
XLA Modules:
  0.0 41.9 jit_solution(17917125614974378511)
XLA Ops:
  0.6 39.3 %shard_map.185 = (bf16[64,1024]{1,0:T(8,128)(2,1)}, f32[2,64,2048]{2,1,0:T(8,128)}) custom-call(bf16[64,1024]{1,0:T(8,128)(2,1)} %x_in.1, s32[4,64]{1,0:T(4,128)} %bitcast.22, f32[4,64]{1,0:T(4,128)} %bitcast.23, f32[32,64]{1,0:T(8,128)} %decay_in.1, f32[32,64]{1,0:T(8,128)} %freq_in.1, f32[1,32]{1,0:T(1,128)} %bitcast.25, f32[2,512,64]{2,1,0:T(8,128)} %bitcast.17, ...), custom_call_target="tpu_custom_call" | custom-call | tf_op jit(solution)/shard_map/pallas_call | solution.py:636
  39.9 2.0 %shard_map.186 = (bf16[64,1024]{1,0:T(8,128)(2,1)}, f32[2,64,2048]{2,1,0:T(8,128)}) custom-call(bf16[64,1024]{1,0:T(8,128)(2,1)} %get-tuple-element.4.u_in, f32[2,64,2048]{2,1,0:T(8,128)} %get-tuple-element.5.s_in), custom_call_target="tpu_custom_call" | custom-call | tf_op jit(solution)/shard_map/pallas_call | solution.py:689
